TPU v7x, 32 devices: a whole 2x2x4 slice. The times are simulated.
32 devices in a mesh: rep: 2 (over x), fs: 8 (over z, y), tp: 2 (over core).
Axes of the slice: x: 2, y: 2, z: 4, core: 2. Of those that a mesh axis runs over, the one named last changes fastest.
Arguments:
- stream_in: bfloat16 [16, 768, 2048], P(('rep', 'fs'), None, 'tp'), may hold values from -6 to 6
- mix_gain: float32 [2048], replicated, may hold values from 0.1 to 1.9
- lin_weight: bfloat16 [2048, 2048], P('fs', 'tp'), may hold values from -0.125 to 0.125
- branch_weight: bfloat16 [2048, 2048], P('fs', 'tp'), may hold values from -0.125 to 0.125
- lin_taps: float32 [4, 2048], P(None, 'tp'), may hold values from -3 to 3
- rate_blocks: bfloat16 [16, 128, 128], P('tp'), may hold values from -0.5 to 0.5
- admit_blocks: bfloat16 [16, 128, 128], P('tp'), may hold values from -0.5 to 0.5
- decay_logit: float32 [2048], P('tp'), may hold values from 3.5 to 9
- mix_out_gain: float32 [2048], P('tp'), may hold values from 0.1 to 1.9
- out_weight: bfloat16 [2048, 2048], P('tp', 'fs'), may hold values from -0.125 to 0.125
- ffn_gain: float32 [2048], replicated, may hold values from 0.1 to 1.9
- gate_weight: bfloat16 [2048, 2816], P('fs', 'tp'), may hold values from -0.125 to 0.125
- up_weight: bfloat16 [2048, 2816], P('fs', 'tp'), may hold values from -0.125 to 0.125
- gate_taps: float32 [3, 2816], P(None, 'tp'), may hold values from -3 to 3
- up_taps: float32 [3, 2816], P(None, 'tp'), may hold values from -3 to 3
- down_weight: bfloat16 [2816, 2048], P('tp', 'fs'), may hold values from -0.109375 to 0.109375
Outputs:
- stream_out: bfloat16 [16, 768, 2048], P(('rep', 'fs'), None, 'tp')
All inputs are finite; a program needn't handle non-finite values.
Results may differ from a plain program's by a relative error of at most 0.018.
Values may be sent and summed in bfloat16 or wider, within the bound.
No kernel may reach another device: no remote copies, remote signals or barrier semaphores. Data moves between devices by JAX's collectives and lax.ppermute only.
A program may use at most 128 MiB of HBM per device.

v0:
```python
import functools

import jax
import jax.numpy as jnp
import numpy as np
from jax import lax
from jax.experimental import pallas as pl
from jax.experimental.pallas import tpu as pltpu
from jax.sharding import PartitionSpec as P


EPS = 1e-06
GATE_SCALE = 8.0
TILE = 16
PARTS = 2
BLOCK_ROWS = 768
NORM_UNROLL = 8
SCAN_UNROLL = 3
ACT_UNROLL = 4
F32 = jnp.float32
BF16 = jnp.bfloat16


VMEM = pl.BlockSpec(memory_space=pltpu.VMEM)
SMEM = pl.BlockSpec(memory_space=pltpu.SMEM)
HBM = pl.BlockSpec(memory_space=pltpu.HBM)


def row_block(length):
    return max(b for b in range(TILE, BLOCK_ROWS + 1, TILE) if length % b == 0)


def fetch_rows(order_ref, pieces, wbuf, sems):
    rows = pieces[0].shape[0]
    copies = []
    for k, piece in enumerate(pieces):
        at = pl.multiple_of(order_ref[k] * rows, rows)
        copies.append(pltpu.make_async_copy(piece, wbuf.at[pl.ds(at, rows)], sems.at[k]))
    return copies


def fetch_blocks(order_ref, pieces, wbuf, sems):
    blocks = wbuf.shape[0]
    per = blocks // len(pieces)
    rows = pieces[0].shape[0] // per
    copies = []
    for k in range(blocks):
        source = pieces[k % len(pieces)].at[pl.ds(k // len(pieces) * rows, rows)]
        copies.append(pltpu.make_async_copy(source, wbuf.at[order_ref[k], pl.ds(0, rows)], sems.at[k]))
    return copies


def norm_into(own_ref, peer_ref, gain_ref, normed_ref):
    length, half = own_ref.shape

    def step(i, _):
        at = pl.ds(pl.multiple_of(i * TILE, TILE), TILE)
        own = own_ref[at, :].astype(F32)
        peer = peer_ref[at, :].astype(F32)
        mean_sq = jnp.sum(own * own + peer * peer, axis=1, keepdims=True) * (0.5 / half)
        scale = lax.rsqrt(mean_sq + EPS)
        normed_ref[at, :half] = (own * scale * gain_ref[0:1, :]).astype(BF16)
        normed_ref[at, half:] = (peer * scale * gain_ref[1:2, :]).astype(BF16)
        return 0

    lax.fori_loop(0, length // TILE, step, 0, unroll=NORM_UNROLL)


def fetch_streams(sources, buffers, sems, first):
    copies = []
    for k, (source, buffer) in enumerate(zip(sources, buffers)):
        rows = buffer.shape[0]
        part = source.at[pl.ds(source.shape[0] - rows, rows)]
        copies.append(pltpu.make_async_copy(part, buffer, sems.at[first + k]))
    return copies


def mix_kernel(n_pieces, order_ref, gain_ref, taps_ref, gates_ref, slope_ref, out_gain_ref, *rest):
    n_pieces -= 2
    streams, pieces = rest[:2], rest[2 : n_pieces + 2]
    mixed_ref, own_ref, peer_ref, normed_ref, wbuf, linear_ref, branch_ref, filt_ref, gate_ref, sems = rest[
        n_pieces + 2 :
    ]
    stream_copies = fetch_streams(streams, (own_ref, peer_ref), sems, n_pieces)
    copies = fetch_rows(order_ref, pieces, wbuf, sems)
    for copy in stream_copies + copies:
        copy.start()
    for copy in stream_copies:
        copy.wait()
    length, width = mixed_ref.shape
    block_count, block, _ = gates_ref.shape
    taps = taps_ref.shape[0]
    norm_into(own_ref, peer_ref, gain_ref, normed_ref)
    for copy in copies:
        copy.wait()
    linear_ref[0:8, :] = jnp.zeros((8, width), F32)
    rows = row_block(length)

    def project(m, _):
        at = pl.multiple_of(m * rows, rows)
        both = jnp.dot(normed_ref[pl.ds(at, rows), :], wbuf[...], preferred_element_type=F32).astype(BF16)
        linear_ref[pl.ds(pl.multiple_of(at + 8, 8), rows), :] = both[:, :width].astype(F32)
        branch_ref[pl.ds(at, rows), :] = both[:, width:]
        return 0

    lax.fori_loop(0, length // rows, project, 0)

    def convolve(i, _):
        at = pl.multiple_of(i * TILE, TILE)
        window = linear_ref[pl.ds(at, TILE + 8), :]
        total = window[9 - taps : 9 - taps + TILE] * taps_ref[0:1, :]
        for j in range(1, taps):
            total = total + window[9 - taps + j : 9 - taps + j + TILE] * taps_ref[j : j + 1, :]
        filt_ref[pl.ds(at, TILE), :] = total
        return 0

    lax.fori_loop(0, length // TILE, convolve, 0, unroll=2)

    def gates(m, _):
        at = pl.ds(pl.multiple_of(m * rows, rows), rows)
        for b in range(block_count):
            piece = filt_ref[at, b * block : (b + 1) * block].astype(BF16)
            gate_ref[at, 2 * b * block : 2 * (b + 1) * block] = jnp.dot(
                piece, gates_ref[b], preferred_element_type=F32
            )
        return 0

    lax.fori_loop(0, length // rows, gates, 0)
    row = lax.broadcasted_iota(jnp.int32, (8, block), 0)

    def scan(i, carry):
        at = pl.ds(pl.multiple_of(i * TILE, TILE), TILE)
        ends = []
        for b in range(block_count):
            cols = slice(b * block, (b + 1) * block)
            filtered = filt_ref[at, cols]
            rate = jax.nn.sigmoid(gate_ref[at, 2 * b * block : (2 * b + 1) * block])
            admit = jax.nn.sigmoid(gate_ref[at, (2 * b + 1) * block : 2 * (b + 1) * block])
            log_decay = rate * slope_ref[0:1, cols]
            fall = 1.0 / 120 + log_decay * (1.0 / 720)
            for coef in (1.0 / 24, 1.0 / 6, 0.5, 1.0):
                fall = coef + log_decay * fall
            fall = log_decay * fall
            decay = 1.0 + fall
            driven = jnp.sqrt(-fall * (2.0 + fall)) * admit * filtered
            last = carry[b]
            states = []
            for part in range(TILE // 8):
                a = decay[part * 8 : part * 8 + 8]
                d = driven[part * 8 : part * 8 + 8]
                for shift in (1, 2, 4):
                    keep = row >= shift
                    d = jnp.where(keep, a * pltpu.roll(d, shift, 0) + d, d)
                    a = jnp.where(keep, a * pltpu.roll(a, shift, 0), a)
                h = a * last + d
                last = jnp.broadcast_to(h[7:8, :], (8, block))
                states.append(h)
            ends.append(last)
            x = branch_ref[at, cols].astype(F32)
            gelu = 0.5 * x * (1.0 + jnp.tanh(0.7978845608028654 * (x + 0.044715 * x * x * x)))
            gated = jnp.concatenate(states, axis=0) * gelu
            mean_sq = jnp.mean(gated * gated, axis=1, keepdims=True)
            mixed_ref[at, cols] = (gated * lax.rsqrt(mean_sq + EPS) * out_gain_ref[0:1, cols]).astype(BF16)
        return tuple(ends)

    zero = jnp.zeros((8, block), F32)
    lax.fori_loop(0, length // TILE, scan, (zero,) * block_count, unroll=SCAN_UNROLL)


def add_kernel(starts, *refs):
    out_ref = refs[-1]

    def step(i, _):
        at = pl.multiple_of(i * TILE, TILE)
        total = None
        for start, ref in zip(starts, refs):
            term = ref[pl.ds(pl.multiple_of(start + at, TILE), TILE), :].astype(F32)
            total = term if total is None else total + term
        out_ref[pl.ds(at, TILE), :] = total.astype(BF16)
        return 0

    lax.fori_loop(0, out_ref.shape[0] // TILE, step, 0, unroll=2)


def ffn_kernel(halo, chunks, n_pieces, order_ref, gain_ref, taps_ref, *rest):
    if halo:
        before_ref, rest = rest[0], rest[1:]
    n_streams = 2 * chunks
    n_pieces -= n_streams
    streams, pieces = rest[:n_streams], rest[n_streams : n_pieces + n_streams]
    hidden_ref, after_ref, own_ref, peer_ref, normed_ref, wbuf, pre_ref, sems = rest[n_pieces + n_streams :]
    buffers = []
    for k, stream in enumerate(streams):
        rows = stream.shape[0]
        buffers.append((own_ref, peer_ref)[k // chunks].at[pl.ds(k % chunks * rows, rows)])
    stream_copies = fetch_streams(streams, buffers, sems, n_pieces)
    copies = fetch_rows(order_ref, pieces, wbuf, sems)
    for copy in stream_copies + copies:
        copy.start()
    for copy in stream_copies:
        copy.wait()
    length = own_ref.shape[0]
    width = wbuf.shape[1]
    taps = taps_ref.shape[0]
    whole = width // 256
    norm_into(own_ref, peer_ref, gain_ref, normed_ref)
    for copy in copies:
        copy.wait()
    rows = row_block(length)
    pre_ref[0:8, :] = before_ref[...] if halo else jnp.zeros((8, width), F32)
    low = lax.broadcasted_iota(jnp.int32, (TILE, 128), 1) < 64

    def project(m, _):
        at = pl.multiple_of(m * rows, rows)
        pre = jnp.dot(normed_ref[pl.ds(at, rows), :], wbuf[...], preferred_element_type=F32)
        pre_ref[8 : 8 + rows, :] = pre.astype(BF16).astype(F32)

        def activate(i, _):
            r = pl.multiple_of(i * TILE, TILE)

            def conv(col):
                cols = slice(col, col + 128)
                window = pre_ref[pl.ds(r, TILE + 8), cols]
                total = window[9 - taps : 9 - taps + TILE] * taps_ref[0:1, cols]
                for j in range(1, taps):
                    total = total + window[9 - taps + j : 9 - taps + j + TILE] * taps_ref[j : j + 1, cols]
                return total

            out = pl.ds(pl.multiple_of(at + r, TILE), TILE)
            for b in range(whole):
                hidden = jax.nn.silu(conv(b * 128)) * conv((whole + b) * 128)
                hidden_ref[out, b * 128 : (b + 1) * 128] = hidden.astype(BF16)
            if width % 256:
                both = conv(2 * whole * 128)
                hidden = jnp.where(low, jax.nn.silu(both) * pltpu.roll(both, 64, 1), 0.0)
                hidden_ref[out, whole * 128 : (whole + 1) * 128] = hidden.astype(BF16)
            return 0

        lax.fori_loop(0, rows // TILE, activate, 0, unroll=ACT_UNROLL)
        pre_ref[0:8, :] = pre_ref[rows : rows + 8, :]
        return 0

    lax.fori_loop(0, length // rows, project, 0)
    after_ref[...] = pre_ref[0:8, :]


def out_kernel(parts, n_pieces, order_ref, left_ref, *rest):
    pieces = rest[:n_pieces]
    keeps, sends = rest[n_pieces : n_pieces + parts], rest[n_pieces + parts : n_pieces + 2 * parts]
    wbuf, sems = rest[n_pieces + 2 * parts :]
    copies = fetch_blocks(order_ref, pieces, wbuf, sems)
    for copy in copies:
        copy.start()
    blocks, padded, width = wbuf.shape
    depth = pieces[0].shape[0] * len(pieces) // blocks
    if padded > depth:
        wbuf[:, depth:, :] = jnp.zeros((blocks, padded - depth, width), BF16)
    length = keeps[0].shape[0]
    rows = row_block(length)
    for copy in copies:
        copy.wait()
    for part in range(parts):

        def step(m, _):
            at = pl.multiple_of(m * rows, rows)
            left = left_ref[pl.ds(pl.multiple_of(part * length + at, rows), rows), :]
            for j in range(blocks):
                total = jnp.dot(left, wbuf[j], preferred_element_type=F32).astype(BF16)
                target = (keeps if j < blocks // 2 else sends)[part]
                col = (j % (blocks // 2)) * width
                target[pl.ds(at, rows), col : col + width] = total
            return 0

        lax.fori_loop(0, length // rows, step, 0)


def call(kernel, outs, scratch, limit_mib, flops, operands, pieces, copies=None):
    specs = [SMEM] + [VMEM] * (len(operands) - 1) + [HBM] * len(pieces)
    return pl.pallas_call(
        functools.partial(kernel, len(pieces)),
        out_shape=outs,
        in_specs=specs,
        out_specs=jax.tree.map(lambda _: VMEM, outs),
        scratch_shapes=scratch + [pltpu.SemaphoreType.DMA((copies or len(pieces),))],
        compiler_params=pltpu.CompilerParams(vmem_limit_bytes=limit_mib * 1024 * 1024),
        cost_estimate=pl.CostEstimate(flops=flops, bytes_accessed=2**22, transcendentals=0),
    )(*operands, *pieces)


def line_ring(n):
    return [0] + list(range(1, n, 2)) + [i for i in range(n - 1, 0, -1) if i % 2 == 0]


def piece_table(n_fs):
    outer = n_fs // 2
    ring = line_ring(outer)
    table = np.zeros((n_fs, 2, n_fs), np.int32)
    for f in range(n_fs):
        z, y = divmod(f, 2)
        found = [ring[(ring.index(z) - k) % outer] for k in range(outer)]
        owners = [q * 2 + y for q in found] + [q * 2 + 1 - y for q in found]
        for c in range(2):
            for k, owner in enumerate(owners):
                half, inside = divmod(owner, n_fs // 2)
                table[f, c, k] = (half ^ c) * (n_fs // 2) + inside
    return table.reshape(n_fs * 2, n_fs)


def local(
    n_fs,
    stream_in,
    mix_gain,
    lin_weight,
    branch_weight,
    lin_taps,
    rate_blocks,
    admit_blocks,
    decay_logit,
    mix_out_gain,
    out_weight,
    ffn_gain,
    gate_weight,
    up_weight,
    gate_taps,
    up_taps,
    down_weight,
):
    outer = n_fs // 2
    ring = line_ring(outer)
    ring_pairs = [
        (ring[p] * 2 + y, ring[(p + 1) % outer] * 2 + y) for p in range(outer) for y in range(2)
    ]
    back_pairs = [(b, a) for a, b in ring_pairs]
    swap_pairs = [(f, f ^ 1) for f in range(n_fs)]
    flip = [(0, 1), (1, 0)]

    def across(value):
        return lax.ppermute(value, "rep", flip)

    def partner(value):
        return lax.ppermute(value, "tp", flip)

    def around(own, ahead=outer // 2):
        found = {0: own}
        for k in range(1, ahead + 1):
            found[k] = lax.ppermute(found[k - 1], "fs", ring_pairs)
        for k in range(outer - 1, ahead, -1):
            found[k] = lax.ppermute(found[(k + 1) % outer], "fs", back_pairs)
        return [found[k] for k in range(outer)]

    def gather_z_first(own, ahead=outer // 2):
        found = around(own, ahead)
        return found + [lax.ppermute(q, "fs", swap_pairs) for q in found]

    def gather_y_first(own):
        return around(jnp.concatenate([own, lax.ppermute(own, "fs", swap_pairs)], axis=0))

    x = lax.axis_index("rep")
    c = lax.axis_index("tp")
    f = lax.axis_index("fs")
    order = jnp.asarray(piece_table(n_fs))[f * 2 + c]

    def half_of(value, axis):
        size = value.shape[axis] // 2
        return lax.dynamic_slice_in_dim(value, x * size, size, axis)

    own = stream_in[0]
    length, half = own.shape
    part = length // PARTS
    channels = lin_weight.shape[1] // 2
    units = gate_weight.shape[1] // 2
    full = units // 128 * 128

    def interleave(gate, up):
        gate, up = half_of(gate, 1), half_of(up, 1)
        return jnp.concatenate([gate[:, :full], up[:, :full], gate[:, full:], up[:, full:]], axis=1)

    both = jnp.concatenate([half_of(lin_weight, 1), half_of(branch_weight, 1)], axis=1)
    mix_pieces = gather_z_first(both, outer - 1)
    other = across(own)
    own_peer = partner(own)
    other_peer = partner(other)
    out_pieces = gather_z_first(half_of(out_weight, 0))
    ffn_pieces = gather_z_first(interleave(gate_weight, up_weight))
    down_pieces = gather_y_first(half_of(down_weight, 0))

    gates = jnp.concatenate([half_of(rate_blocks, 0), half_of(admit_blocks, 0)], axis=2)
    slope = -GATE_SCALE * jax.nn.softplus(-half_of(decay_logit, 0))[None]
    out_gain = half_of(mix_out_gain, 0)[None]
    taps = half_of(lin_taps, 1)
    gain = jnp.where(c == 0, mix_gain.reshape(2, half), mix_gain.reshape(2, half)[::-1])
    gain2 = jnp.where(c == 0, ffn_gain.reshape(2, half), ffn_gain.reshape(2, half)[::-1])
    ffn_taps = interleave(gate_taps, up_taps)
    padded_units = -(-units // 128) * 128

    def mix(stream, peer):
        return call(
            mix_kernel,
            jax.ShapeDtypeStruct((length, channels), BF16),
            [
                pltpu.VMEM((length, half), BF16),
                pltpu.VMEM((length, half), BF16),
                pltpu.VMEM((length, 2 * half), BF16),
                pltpu.VMEM((2 * half, 2 * channels), BF16),
                pltpu.VMEM((length + 8, channels), F32),
                pltpu.VMEM((length, channels), BF16),
                pltpu.VMEM((length, channels), F32),
                pltpu.VMEM((length, 2 * channels), F32),
            ],
            30,
            length * 2 * half * 2 * channels * 2,
            [order, gain, taps, gates, slope, out_gain],
            [stream, peer] + mix_pieces,
        )

    def project(left, pieces):
        rows, depth = left.shape
        parts = rows // part
        sums = [jax.ShapeDtypeStruct((part, half), BF16)] * (2 * parts)
        outs = call(
            functools.partial(out_kernel, parts),
            sums,
            [pltpu.VMEM((n_fs, depth, pieces[0].shape[1]), BF16)],
            16,
            rows * depth * 2 * half * 2,
            [order, left],
            pieces,
            n_fs,
        )
        return outs[:parts], outs[parts:]

    def ffn(owns, peers, before):
        width = 2 * units
        rows = len(owns) * part
        halo = [] if before is None else [before]
        return call(
            functools.partial(ffn_kernel, bool(halo), len(owns)),
            (jax.ShapeDtypeStruct((rows, padded_units), BF16), jax.ShapeDtypeStruct((8, width), F32)),
            [
                pltpu.VMEM((rows, half), BF16),
                pltpu.VMEM((rows, half), BF16),
                pltpu.VMEM((rows, 2 * half), BF16),
                pltpu.VMEM((2 * half, width), BF16),
                pltpu.VMEM((row_block(rows) + 8, width), F32),
            ],
            28,
            rows * 2 * half * width * 2,
            [order, gain2, ffn_taps] + halo,
            owns + peers + ffn_pieces,
        )

    def add(*terms):
        starts = [t[1] if isinstance(t, tuple) else 0 for t in terms]
        arrays = [t[0] if isinstance(t, tuple) else t for t in terms]
        return pl.pallas_call(
            functools.partial(add_kernel, starts),
            out_shape=jax.ShapeDtypeStruct((part, half), BF16),
            in_specs=[VMEM] * len(arrays),
            out_specs=VMEM,
            compiler_params=pltpu.CompilerParams(vmem_limit_bytes=12 * 1024 * 1024),
            cost_estimate=pl.CostEstimate(flops=part * half * len(arrays), bytes_accessed=2**21, transcendentals=0),
        )(*arrays)

    mixed_other = mix(other, other_peer)
    keep_other, send_other = project(mixed_other, out_pieces)
    sent = []
    for i in range(PARTS):
        value = add(keep_other[i], partner(send_other[i]))
        sent.append(across(value))
    mixed_own = mix(own, own_peer)
    keep_own, send_own = project(mixed_own, out_pieces)
    middle, middle_peer, middle_other = [], [], []
    for i in range(PARTS):
        value = add((own, i * part), keep_own[i], partner(send_own[i]), sent[i])
        middle.append(value)
        middle_other.append(across(value))
        middle_peer.append(partner(value))
    other_middle_peer = [partner(value) for value in middle_other]

    tail, sent = None, []
    for i in range(PARTS):
        hidden, tail = ffn([middle_other[i]], [other_middle_peer[i]], tail)
        keep, send = project(hidden, down_pieces)
        sent.append(across(add(keep[0], partner(send[0]))))
    hidden, _ = ffn(middle, middle_peer, None)
    keeps, sends = project(hidden, down_pieces)
    result = []
    for i in range(PARTS):
        terms = [middle[i], keeps[i], partner(sends[i]), sent[i]]
        result.append(functools.reduce(jnp.add, [t.astype(F32) for t in terms]).astype(BF16))
    return jnp.concatenate(result, axis=0)[None]


def solution(mesh):
    placed = (
        P(("rep", "fs"), None, "tp"),
        P(),
        P("fs", "tp"),
        P("fs", "tp"),
        P(None, "tp"),
        P("tp", None, None),
        P("tp", None, None),
        P("tp"),
        P("tp"),
        P("tp", "fs"),
        P(),
        P("fs", "tp"),
        P("fs", "tp"),
        P(None, "tp"),
        P(None, "tp"),
        P("tp", "fs"),
    )

    def body(*args):
        return local(mesh.shape["fs"], *args)

    return jax.shard_map(
        body,
        mesh=mesh,
        in_specs=placed,
        out_specs=P(("rep", "fs"), None, "tp"),
        check_vma=False,
    )
```

profile of v0, /device:TPU:28, one launch (start us, length us, event | category | flops | bytes accessed | tf_op | source)
XLA Modules:
  0.0 333.5 jit_solution(5443209620996371690)
XLA Ops:
  0.0 1.6 collective-permute-start.16
  1.6 1.1 constant_dynamic-slice_fusion.10
  3.3 13.8 %collective-permute-done.1.rest_3_ = bf16[256,1024]{1,0:T(8,128)(2,1)S(1)} collective-permute-done((bf16[256,1024]{1,0:T(8,128)(2,1)S(1)}, bf16[256,1024]{1,0:T(8,128)(2,1)S(1)}, u32[]{:S(2)}, u32[]{:S(2)}) %collective-permute-start.1) | collective-permute-done | bytes 524320 | tf_op jit(solution)/shard_map/ppermute | solution.py:346
  17.1 19.4 %collective-permute-done.16.rest_0_ = bf16[768,1024]{1,0:T(8,128)(2,1)} collective-permute-done((bf16[768,1024]{1,0:T(8,128)(2,1)}, bf16[768,1024]{1,0:T(8,128)(2,1)}, u32[]{:S(2)}, u32[]{:S(2)}) %collective-permute-start.16) | collective-permute-done | bytes 1572896 | tf_op jit(solution)/shard_map/ppermute | solution.py:338
  37.6 2.5 collective-permute-start.10
  40.1 12.3 %collective-permute-done.8.rest_1_ = bf16[512,256]{1,0:T(8,128)(2,1)S(1)} collective-permute-done((bf16[512,256]{1,0:T(8,128)(2,1)S(1)}, bf16[512,256]{1,0:T(8,128)(2,1)S(1)}, u32[]{:S(2)}, u32[]{:S(2)}) %collective-permute-start.8) | collective-permute-done | bytes 262176 | tf_op jit(solution)/shard_map/ppermute | solution.py:346
  52.4 0.7 copy-done.28
  54.1 14.7 %collective-permute-done.9.rest_2_ = bf16[512,256]{1,0:T(8,128)(2,1)} collective-permute-done((bf16[512,256]{1,0:T(8,128)(2,1)S(1)}, bf16[512,256]{1,0:T(8,128)(2,1)}, u32[]{:S(2)}, u32[]{:S(2)}) %collective-permute-start.9) | collective-permute-done | bytes 262176 | tf_op jit(solution)/shard_map/ppermute | solution.py:346
  69.4 1.5 collective-permute-start.7
  70.9 0.7 fusion.1.order_ref
  71.6 1.0 constant_dynamic-slice_fusion.12
  73.2 10.7 %collective-permute-done.6.rest_8_ = bf16[256,1024]{1,0:T(8,128)(2,1)S(1)} collective-permute-done((bf16[256,1024]{1,0:T(8,128)(2,1)}, bf16[256,1024]{1,0:T(8,128)(2,1)S(1)}, u32[]{:S(2)}, u32[]{:S(2)}) %collective-permute-start.6) | collective-permute-done | bytes 524320 | tf_op jit(solution)/shard_map/ppermute | solution.py:353
  84.4 10.7 %collective-permute-done.7.rest_9_ = bf16[256,1024]{1,0:T(8,128)(2,1)S(1)} collective-permute-done((bf16[256,1024]{1,0:T(8,128)(2,1)}, bf16[256,1024]{1,0:T(8,128)(2,1)S(1)}, u32[]{:S(2)}, u32[]{:S(2)}) %collective-permute-start.7) | collective-permute-done | bytes 524320 | tf_op jit(solution)/shard_map/ppermute | solution.py:353
  95.6 1.5 collective-permute-start.13
  97.1 1.0 copy-done.27
  98.2 14.0 %shard_map.165.left_ref = bf16[768,512]{1,0:T(8,128)(2,1)S(1)} custom-call(s32[8]{0:T(128)S(1)} %fusion.1.order_ref, f32[2,1024]{1,0:T(2,128)S(1)} %broadcast_select_fusion.1.gain_ref, f32[4,512]{1,0:T(4,128)S(1)} %constant_dynamic-slice_fusion.14.taps_ref, bf16[4,128,256]{2,1,0:T(8,128)(2,1)S(1)} %pad_maximum_fusion.2.gates_ref, f32[1,512]{1,0:T(1,128)S(1)} %bitcast.14, ...), custom_call_target="tpu_custom_call" | custom-call | flops 3221225472 | bytes 4194304 | tf_op jit(solution)/shard_map/pallas_call | solution.py:279
  112.2 4.1 %collective-permute-done.13.rest_6_ = bf16[512,256]{1,0:T(8,128)(2,1)S(1)} collective-permute-done((bf16[512,256]{1,0:T(8,128)(2,1)}, bf16[512,256]{1,0:T(8,128)(2,1)S(1)}, u32[]{:S(2)}, u32[]{:S(2)}) %collective-permute-start.13) | collective-permute-done | bytes 262176 | tf_op jit(solution)/shard_map/ppermute | solution.py:353
  116.3 4.3 %shard_map.166 = (bf16[384,1024]{1,0:T(8,128)(2,1)S(1)}, bf16[384,1024]{1,0:T(8,128)(2,1)S(1)}, bf16[384,1024]{1,0:T(8,128)(2,1)S(1)}, bf16[384,1024]{1,0:T(8,128)(2,1)}) custom-call(s32[8]{0:T(128)S(1)} %fusion.1.order_ref, bf16[768,512]{1,0:T(8,128)(2,1)S(1)} %shard_map.165.left_ref, bf16[512,256]{1,0:T(8,128)(2,1)S(1)} %constant_dynamic-slice_fusion.9.rest_0_, ...), custom_call_target="tpu_custom_call" | custom-call | flops 1610612736 | bytes 4194304 | tf_op jit(solution)/shard_map/pallas_call | solution.py:279
  120.6 0.9 copy-done.10
  121.5 13.6 %shard_map.163.left_ref = bf16[768,512]{1,0:T(8,128)(2,1)S(1)} custom-call(s32[8]{0:T(128)S(1)} %fusion.1.order_ref, f32[2,1024]{1,0:T(2,128)S(1)} %broadcast_select_fusion.1.gain_ref, f32[4,512]{1,0:T(4,128)S(1)} %constant_dynamic-slice_fusion.14.taps_ref, bf16[4,128,256]{2,1,0:T(8,128)(2,1)S(1)} %pad_maximum_fusion.2.gates_ref, f32[1,512]{1,0:T(1,128)S(1)} %bitcast.15, ...), custom_call_target="tpu_custom_call" | custom-call | flops 3221225472 | bytes 4194304 | tf_op jit(solution)/shard_map/pallas_call | solution.py:279
  135.7 3.9 %shard_map.164 = (bf16[384,1024]{1,0:T(8,128)(2,1)S(1)}, bf16[384,1024]{1,0:T(8,128)(2,1)S(1)}, bf16[384,1024]{1,0:T(8,128)(2,1)}, bf16[384,1024]{1,0:T(8,128)(2,1)S(1)}) custom-call(s32[8]{0:T(128)S(1)} %fusion.1.order_ref, bf16[768,512]{1,0:T(8,128)(2,1)S(1)} %shard_map.163.left_ref, bf16[512,256]{1,0:T(8,128)(2,1)S(1)} %constant_dynamic-slice_fusion.9.rest_0_, ...), custom_call_target="tpu_custom_call" | custom-call | flops 1610612736 | bytes 4194304 | tf_op jit(solution)/shard_map/pallas_call | solution.py:279
  139.6 0.9 copy-done.4
  140.5 0.9 copy-done.6
  141.4 1.2 shard_map.167
  142.5 1.5 collective-permute-start.19
  144.0 2.3 constant_dynamic-slice_fusion
  146.6 1.0 constant_dynamic-slice_fusion.5
  147.5 2.0 concatenate.21.rest_4_.rest_2_.rest_3_
  149.6 1.2 copy-done.11
  150.8 1.5 shard_map.169
  152.9 0.9 copy-done.8
  154.3 9.0 %collective-permute-done.19.refs_3_ = bf16[384,1024]{1,0:T(8,128)(2,1)} collective-permute-done((bf16[384,1024]{1,0:T(8,128)(2,1)}, bf16[384,1024]{1,0:T(8,128)(2,1)}, u32[]{:S(2)}, u32[]{:S(2)}) %collective-permute-start.19) | collective-permute-done | bytes 786464 | tf_op jit(solution)/shard_map/ppermute | solution.py:338
  163.3 1.1 copy-done.9
  164.4 1.6 shard_map.168.rest_0_
  166.1 1.6 collective-permute-start.37
  167.7 16.9 %collective-permute-done.25.rest_5_.rest_3_.rest_4_ = bf16[256,1408]{1,0:T(8,128)(2,1)} collective-permute-done((bf16[256,1408]{1,0:T(8,128)(2,1)}, bf16[256,1408]{1,0:T(8,128)(2,1)}, u32[]{:S(2)}, u32[]{:S(2)}) %collective-permute-start.25) | collective-permute-done | bytes 720928 | tf_op jit(solution)/shard_map/ppermute | solution.py:346
  185.2 1.6 shard_map.170.rest_1_
  186.8 0.6 collective-permute-start.42
  187.4 14.6 %collective-permute-done.28.rest_8_.rest_6_.rest_7_ = bf16[256,1408]{1,0:T(8,128)(2,1)S(1)} collective-permute-done((bf16[256,1408]{1,0:T(8,128)(2,1)S(1)}, bf16[256,1408]{1,0:T(8,128)(2,1)S(1)}, u32[]{:S(2)}, u32[]{:S(2)}) %collective-permute-start.28) | collective-permute-done | bytes 720928 | tf_op jit(solution)/shard_map/ppermute | solution.py:353
  202.1 0.9 copy-done.20
  203.4 1.6 collective-permute-done.33.rest_1_
  205.0 1.5 collective-permute-start.31
  206.5 12.2 %collective-permute-done.26.rest_6_.rest_4_.rest_5_ = bf16[256,1408]{1,0:T(8,128)(2,1)} collective-permute-done((bf16[256,1408]{1,0:T(8,128)(2,1)}, bf16[256,1408]{1,0:T(8,128)(2,1)}, u32[]{:S(2)}, u32[]{:S(2)}) %collective-permute-start.26) | collective-permute-done | bytes 720928 | tf_op jit(solution)/shard_map/ppermute | solution.py:346
  218.7 1.5 collective-permute-start.30
  220.6 1.5 collective-permute-done.29.rest_9_.rest_7_.rest_8_
  222.1 0.9 copy-done.23
  223.0 14.7 %collective-permute-done.31.rest_11_.rest_9_.rest_10_ = bf16[256,1408]{1,0:T(8,128)(2,1)} collective-permute-done((bf16[256,1408]{1,0:T(8,128)(2,1)}, bf16[256,1408]{1,0:T(8,128)(2,1)}, u32[]{:S(2)}, u32[]{:S(2)}) %collective-permute-start.31) | collective-permute-done | bytes 720928 | tf_op jit(solution)/shard_map/ppermute | solution.py:353
  237.9 13.0 %collective-permute-done.30.rest_10_.rest_8_.rest_9_ = bf16[256,1408]{1,0:T(8,128)(2,1)} collective-permute-done((bf16[256,1408]{1,0:T(8,128)(2,1)}, bf16[256,1408]{1,0:T(8,128)(2,1)}, u32[]{:S(2)}, u32[]{:S(2)}) %collective-permute-start.30) | collective-permute-done | bytes 720928 | tf_op jit(solution)/shard_map/ppermute | solution.py:353
  251.4 1.1 copy-done.13
  252.5 1.1 copy-done.21
  253.6 1.1 copy-done.24
  254.7 7.1 %shard_map.173 = (bf16[384,768]{1,0:T(8,128)(2,1)S(1)}, f32[8,1408]{1,0:T(8,128)S(1)}) custom-call(s32[8]{0:T(128)S(1)} %fusion.1.order_ref, f32[2,1024]{1,0:T(2,128)S(1)} %broadcast_select_fusion.gain_ref, f32[3,1408]{1,0:T(4,128)S(1)} %concatenate.20.taps_ref, bf16[384,1024]{1,0:T(8,128)(2,1)} %collective-permute-done.37.rest_0_, ...), custom_call_target="tpu_custom_call" | custom-call | flops 2214592512 | bytes 4194304 | tf_op jit(solution)/shard_map/pallas_call | solution.py:279
  261.8 7.8 %shard_map.176 = (bf16[384,768]{1,0:T(8,128)(2,1)S(1)}, f32[8,1408]{1,0:T(8,128)}) custom-call(s32[8]{0:T(128)S(1)} %fusion.1.order_ref, f32[2,1024]{1,0:T(2,128)S(1)} %broadcast_select_fusion.gain_ref, f32[3,1408]{1,0:T(4,128)S(1)} %concatenate.20.taps_ref, f32[8,1408]{1,0:T(8,128)S(1)} %get-tuple-element.41.rest_0_, ...), custom_call_target="tpu_custom_call" | custom-call | flops 2214592512 | bytes 4194304 | tf_op jit(solution)/shard_map/pallas_call | solution.py:279
  269.7 3.7 %shard_map.177 = (bf16[384,1024]{1,0:T(8,128)(2,1)S(1)}, bf16[384,1024]{1,0:T(8,128)(2,1)S(1)}) custom-call(s32[8]{0:T(128)S(1)} %fusion.1.order_ref, bf16[384,768]{1,0:T(8,128)(2,1)S(1)} %get-tuple-element.42.left_ref, bf16[1408,256]{1,0:T(8,128)(2,1)S(1)} %copy-done.16, bf16[1408,256]{1,0:T(8,128)(2,1)S(1)} %copy-done.19, ...), custom_call_target="tpu_custom_call" | custom-call | flops 1207959552 | bytes 4194304 | tf_op jit(solution)/shard_map/pallas_call | solution.py:279
  273.5 3.7 %shard_map.174 = (bf16[384,1024]{1,0:T(8,128)(2,1)S(1)}, bf16[384,1024]{1,0:T(8,128)(2,1)S(1)}) custom-call(s32[8]{0:T(128)S(1)} %fusion.1.order_ref, bf16[384,768]{1,0:T(8,128)(2,1)S(1)} %get-tuple-element.36.left_ref, bf16[1408,256]{1,0:T(8,128)(2,1)S(1)} %copy-done.16, bf16[1408,256]{1,0:T(8,128)(2,1)S(1)} %copy-done.19, ...), custom_call_target="tpu_custom_call" | custom-call | flops 1207959552 | bytes 4194304 | tf_op jit(solution)/shard_map/pallas_call | solution.py:279
  277.8 11.6 %shard_map.171 = (bf16[768,768]{1,0:T(8,128)(2,1)S(1)}, f32[8,1408]{1,0:T(8,128)}) custom-call(s32[8]{0:T(128)S(1)} %fusion.1.order_ref, f32[2,1024]{1,0:T(2,128)S(1)} %broadcast_select_fusion.gain_ref, f32[3,1408]{1,0:T(4,128)S(1)} %concatenate.20.taps_ref, bf16[384,1024]{1,0:T(8,128)(2,1)S(1)} %shard_map.168.rest_0_, bf16[384,1024]{1,0:T(8,128)(2,1)S(1)} %copy-done.3, ...), custom_call_target="tpu_custom_call" | custom-call | flops 4429185024 | bytes 4194304 | tf_op jit(solution)/shard_map/pallas_call | solution.py:279
  289.4 5.0 %shard_map.172 = (bf16[384,1024]{1,0:T(8,128)(2,1)S(1)}, bf16[384,1024]{1,0:T(8,128)(2,1)S(1)}, bf16[384,1024]{1,0:T(8,128)(2,1)S(1)}, bf16[384,1024]{1,0:T(8,128)(2,1)S(1)}) custom-call(s32[8]{0:T(128)S(1)} %fusion.1.order_ref, bf16[768,768]{1,0:T(8,128)(2,1)S(1)} %get-tuple-element.33.left_ref, bf16[1408,256]{1,0:T(8,128)(2,1)S(1)} %copy-done.16, ...), custom_call_target="tpu_custom_call" | custom-call | flops 2415919104 | bytes 4194304 | tf_op jit(solution)/shard_map/pallas_call | solution.py:279
  294.8 0.6 collective-permute-start.45
  295.8 1.6 collective-permute-start.40
  297.4 17.9 %collective-permute-done.45 = bf16[384,1024]{1,0:T(8,128)(2,1)S(1)} collective-permute-done((bf16[384,1024]{1,0:T(8,128)(2,1)S(1)}, bf16[384,1024]{1,0:T(8,128)(2,1)S(1)}, u32[]{:S(2)}, u32[]{:S(2)}) %collective-permute-start.45) | collective-permute-done | bytes 786464 | tf_op jit(solution)/shard_map/ppermute | solution.py:338
  315.3 0.6 add_convert_fusion
  315.9 15.7 %collective-permute-done.40 = bf16[384,1024]{1,0:T(8,128)(2,1)S(1)} collective-permute-done((bf16[384,1024]{1,0:T(8,128)(2,1)S(1)}, bf16[384,1024]{1,0:T(8,128)(2,1)S(1)}, u32[]{:S(2)}, u32[]{:S(2)}) %collective-permute-start.40) | collective-permute-done | bytes 786464 | tf_op jit(solution)/shard_map/ppermute | solution.py:338
  331.6 0.6 add_convert_fusion.1
  332.2 1.3 maximum_bitcast_fusion
  (146 shorter events, 10.4 us)
Async XLA Ops:
  0.0 152.8 %copy-start = (bf16[1408,256]{1,0:T(8,128)(2,1)S(1)}, bf16[1408,256]{1,0:T(8,128)(2,1)}, u32[]{:S(2)}) copy-start(bf16[1408,256]{1,0:T(8,128)(2,1)} %param.32) | copy-start | bytes 2162692
  0.0 52.4 %copy-start.1 = (bf16[1,768,1024]{2,1,0:T(8,128)(2,1)S(1)}, bf16[1,768,1024]{2,1,0:T(8,128)(2,1)}, u32[]{:S(2)}) copy-start(bf16[1,768,1024]{2,1,0:T(8,128)(2,1)} %param.17) | copy-start | bytes 4718596
  0.0 53.1 %copy-start.31 = (f32[2048]{0:T(1024)S(1)}, f32[2048]{0:T(1024)}, u32[]{:S(2)}) copy-start(f32[2048]{0:T(1024)} %param.18) | copy-start | bytes 24580
  0.0 53.4 %copy-start.36 = (f32[1024]{0:T(1024)S(1)}, f32[1024]{0:T(1024)}, u32[]{:S(2)}) copy-start(f32[1024]{0:T(1024)} %param.25) | copy-start | bytes 12292
  0.0 53.4 %copy-start.37 = (f32[1024]{0:T(1024)S(1)}, f32[1024]{0:T(1024)}, u32[]{:S(2)}) copy-start(f32[1024]{0:T(1024)} %param.24) | copy-start | bytes 12292
  0.0 36.5 %collective-permute-start.16 = (bf16[768,1024]{1,0:T(8,128)(2,1)}, bf16[768,1024]{1,0:T(8,128)(2,1)}, u32[]{:S(2)}, u32[]{:S(2)}) collective-permute-start(bf16[768,1024]{1,0:T(8,128)(2,1)} %bitcast.7), channel_id=1, source_target_pairs={{0,16},{16,0},{1,17},{17,1},{2,18},{18,2},{3,19},{19,3},{4,20},{20... | collective-permute-start | bytes 4718600 | tf_op jit(solution)/shard_map/ppermute | solution.py:338
  1.6 35.0 %copy-start.30 = (bf16[1024,256]{1,0:T(8,128)(2,1)S(1)}, bf16[1024,256]{1,0:T(8,128)(2,1)}, u32[]{:S(2)}) copy-start(bf16[1024,256]{1,0:T(8,128)(2,1)} %param.26) | copy-start | bytes 1572868
  1.6 52.0 %copy-start.35 = (f32[4,1024]{1,0:T(4,128)S(1)}, f32[4,1024]{1,0:T(4,128)}, u32[]{:S(2)}) copy-start(f32[4,1024]{1,0:T(4,128)} %param.21) | copy-start | bytes 49156
  2.8 14.3 %collective-permute-start.1 = (bf16[256,1024]{1,0:T(8,128)(2,1)S(1)}, bf16[256,1024]{1,0:T(8,128)(2,1)S(1)}, u32[]{:S(2)}, u32[]{:S(2)}) collective-permute-start(bf16[256,1024]{1,0:T(8,128)(2,1)S(1)} %pad_maximum_fusion.1.rest_2_), channel_id=1, source_target_pairs={{0,4},{2,6},{4,12},{6,14},{12,8},{14,10},{8,0},{10,2},{1,5},{3,7},... | collective-permute-start | bytes 1572872 | tf_op jit(solution)/shard_map/ppermute | solution.py:346
  17.1 35.3 %copy-start.26 = (bf16[256,1024]{1,0:T(8,128)(2,1)}, bf16[256,1024]{1,0:T(8,128)(2,1)S(1)}, u32[]{:S(2)}) copy-start(bf16[256,1024]{1,0:T(8,128)(2,1)S(1)} %collective-permute-done.1.rest_3_) | copy-start | bytes 1572868
  17.1 22.9 %collective-permute-start.2 = (bf16[256,1024]{1,0:T(8,128)(2,1)S(1)}, bf16[256,1024]{1,0:T(8,128)(2,1)}, u32[]{:S(2)}, u32[]{:S(2)}) collective-permute-start(bf16[256,1024]{1,0:T(8,128)(2,1)S(1)} %collective-permute-done.1.rest_3_), channel_id=1, source_target_pairs={{0,4},{2,6},{4,12},{6,14},{12,8},{14,10},{8,0},{10,2},{1,5},{3,7},... | collective-permute-start | bytes 1572872 | tf_op jit(solution)/shard_map/ppermute | solution.py:346
  36.5 59.1 %collective-permute-start.17 = (bf16[768,1024]{1,0:T(8,128)(2,1)}, bf16[768,1024]{1,0:T(8,128)(2,1)}, u32[]{:S(2)}, u32[]{:S(2)}) collective-permute-start(bf16[768,1024]{1,0:T(8,128)(2,1)} %collective-permute-done.16.rest_0_), channel_id=1, source_target_pairs={{0,1},{1,0},{2,3},{3,2},{4,5},{5,4},{6,7},{7,6},{8,9},{9,8},{10,11... | collective-permute-start | bytes 4718600 | tf_op jit(solution)/shard_map/ppermute | solution.py:341
  36.6 15.8 %collective-permute-start.8 = (bf16[512,256]{1,0:T(8,128)(2,1)S(1)}, bf16[512,256]{1,0:T(8,128)(2,1)S(1)}, u32[]{:S(2)}, u32[]{:S(2)}) collective-permute-start(bf16[512,256]{1,0:T(8,128)(2,1)S(1)} %constant_dynamic-slice_fusion.9.rest_0_), channel_id=1, source_target_pairs={{0,4},{2,6},{4,12},{6,14},{12,8},{14,10},{8,0},{10,2},{1,5},{3,7},... | collective-permute-start | bytes 786440 | tf_op jit(solution)/shard_map/ppermute | solution.py:346
  37.1 16.5 %collective-permute-start.4 = (bf16[256,1024]{1,0:T(8,128)(2,1)S(1)}, bf16[256,1024]{1,0:T(8,128)(2,1)}, u32[]{:S(2)}, u32[]{:S(2)}) collective-permute-start(bf16[256,1024]{1,0:T(8,128)(2,1)S(1)} %pad_maximum_fusion.1.rest_2_), channel_id=1, source_target_pairs={{0,2},{2,0},{4,6},{6,4},{8,10},{10,8},{12,14},{14,12},{1,3},{3,1},... | collective-permute-start | bytes 1572872 | tf_op jit(solution)/shard_map/ppermute | solution.py:353
  37.6 14.8 %collective-permute-start.10 = (bf16[512,256]{1,0:T(8,128)(2,1)S(1)}, bf16[512,256]{1,0:T(8,128)(2,1)S(1)}, u32[]{:S(2)}, u32[]{:S(2)}) collective-permute-start(bf16[512,256]{1,0:T(8,128)(2,1)S(1)} %constant_dynamic-slice_fusion.9.rest_0_), channel_id=1, source_target_pairs={{4,0},{6,2},{12,4},{14,6},{8,12},{10,14},{0,8},{2,10},{5,1},{7,3},... | collective-permute-start | bytes 786440 | tf_op jit(solution)/shard_map/ppermute | solution.py:348
  40.1 29.3 %collective-permute-start.3 = (bf16[256,1024]{1,0:T(8,128)(2,1)}, bf16[256,1024]{1,0:T(8,128)(2,1)}, u32[]{:S(2)}, u32[]{:S(2)}) collective-permute-start(bf16[256,1024]{1,0:T(8,128)(2,1)} %collective-permute-done.2.rest_4_), channel_id=1, source_target_pairs={{0,4},{2,6},{4,12},{6,14},{12,8},{14,10},{8,0},{10,2},{1,5},{3,7},... | collective-permute-start | bytes 1572872 | tf_op jit(solution)/shard_map/ppermute | solution.py:346
  52.4 69.1 %collective-permute-start = (bf16[768,1024]{1,0:T(8,128)(2,1)S(1)}, bf16[768,1024]{1,0:T(8,128)(2,1)}, u32[]{:S(2)}, u32[]{:S(2)}) collective-permute-start(bf16[768,1024]{1,0:T(8,128)(2,1)S(1)} %bitcast.8), channel_id=1, source_target_pairs={{0,1},{1,0},{2,3},{3,2},{4,5},{5,4},{6,7},{7,6},{8,9},{9,8},{10,11... | collective-permute-start | bytes 4718600 | tf_op jit(solution)/shard_map/ppermute | solution.py:341
  53.1 15.7 %collective-permute-start.9 = (bf16[512,256]{1,0:T(8,128)(2,1)S(1)}, bf16[512,256]{1,0:T(8,128)(2,1)}, u32[]{:S(2)}, u32[]{:S(2)}) collective-permute-start(bf16[512,256]{1,0:T(8,128)(2,1)S(1)} %collective-permute-done.8.rest_1_), channel_id=1, source_target_pairs={{0,4},{2,6},{4,12},{6,14},{12,8},{14,10},{8,0},{10,2},{1,5},{3,7},... | collective-permute-start | bytes 786440 | tf_op jit(solution)/shard_map/ppermute | solution.py:346
  53.6 19.1 %collective-permute-start.5 = (bf16[256,1024]{1,0:T(8,128)(2,1)}, bf16[256,1024]{1,0:T(8,128)(2,1)S(1)}, u32[]{:S(2)}, u32[]{:S(2)}) collective-permute-start(bf16[256,1024]{1,0:T(8,128)(2,1)} %copy-done.26), channel_id=1, source_target_pairs={{0,2},{2,0},{4,6},{6,4},{8,10},{10,8},{12,14},{14,12},{1,3},{3,1},... | collective-permute-start | bytes 1572872 | tf_op jit(solution)/shard_map/ppermute | solution.py:353
  68.9 15.0 %collective-permute-start.6 = (bf16[256,1024]{1,0:T(8,128)(2,1)}, bf16[256,1024]{1,0:T(8,128)(2,1)S(1)}, u32[]{:S(2)}, u32[]{:S(2)}) collective-permute-start(bf16[256,1024]{1,0:T(8,128)(2,1)} %collective-permute-done.2.rest_4_), channel_id=1, source_target_pairs={{0,2},{2,0},{4,6},{6,4},{8,10},{10,8},{12,14},{14,12},{1,3},{3,1},... | collective-permute-start | bytes 1572872 | tf_op jit(solution)/shard_map/ppermute | solution.py:353
  69.4 25.7 %collective-permute-start.7 = (bf16[256,1024]{1,0:T(8,128)(2,1)}, bf16[256,1024]{1,0:T(8,128)(2,1)S(1)}, u32[]{:S(2)}, u32[]{:S(2)}) collective-permute-start(bf16[256,1024]{1,0:T(8,128)(2,1)} %collective-permute-done.3.rest_5_), channel_id=1, source_target_pairs={{0,2},{2,0},{4,6},{6,4},{8,10},{10,8},{12,14},{14,12},{1,3},{3,1},... | collective-permute-start | bytes 1572872 | tf_op jit(solution)/shard_map/ppermute | solution.py:353
  72.6 39.5 %collective-permute-start.11 = (bf16[512,256]{1,0:T(8,128)(2,1)S(1)}, bf16[512,256]{1,0:T(8,128)(2,1)S(1)}, u32[]{:S(2)}, u32[]{:S(2)}) collective-permute-start(bf16[512,256]{1,0:T(8,128)(2,1)S(1)} %constant_dynamic-slice_fusion.9.rest_0_), channel_id=1, source_target_pairs={{0,2},{2,0},{4,6},{6,4},{8,10},{10,8},{12,14},{14,12},{1,3},{3,1},... | collective-permute-start | bytes 786440 | tf_op jit(solution)/shard_map/ppermute | solution.py:353
  83.9 28.3 %collective-permute-start.12 = (bf16[512,256]{1,0:T(8,128)(2,1)S(1)}, bf16[512,256]{1,0:T(8,128)(2,1)S(1)}, u32[]{:S(2)}, u32[]{:S(2)}) collective-permute-start(bf16[512,256]{1,0:T(8,128)(2,1)S(1)} %collective-permute-done.8.rest_1_), channel_id=1, source_target_pairs={{0,2},{2,0},{4,6},{6,4},{8,10},{10,8},{12,14},{14,12},{1,3},{3,1},... | collective-permute-start | bytes 786440 | tf_op jit(solution)/shard_map/ppermute | solution.py:353
  95.1 17.1 %collective-permute-start.14 = (bf16[512,256]{1,0:T(8,128)(2,1)}, bf16[512,256]{1,0:T(8,128)(2,1)S(1)}, u32[]{:S(2)}, u32[]{:S(2)}) collective-permute-start(bf16[512,256]{1,0:T(8,128)(2,1)} %copy-done.28), channel_id=1, source_target_pairs={{0,2},{2,0},{4,6},{6,4},{8,10},{10,8},{12,14},{14,12},{1,3},{3,1},... | collective-permute-start | bytes 786440 | tf_op jit(solution)/shard_map/ppermute | solution.py:353
  95.6 20.6 %collective-permute-start.13 = (bf16[512,256]{1,0:T(8,128)(2,1)}, bf16[512,256]{1,0:T(8,128)(2,1)S(1)}, u32[]{:S(2)}, u32[]{:S(2)}) collective-permute-start(bf16[512,256]{1,0:T(8,128)(2,1)} %collective-permute-done.9.rest_2_), channel_id=1, source_target_pairs={{0,2},{2,0},{4,6},{6,4},{8,10},{10,8},{12,14},{14,12},{1,3},{3,1},... | collective-permute-start | bytes 786440 | tf_op jit(solution)/shard_map/ppermute | solution.py:353
  98.2 18.1 %copy-start.29 = (bf16[512,256]{1,0:T(8,128)(2,1)S(1)}, bf16[512,256]{1,0:T(8,128)(2,1)}, u32[]{:S(2)}) copy-start(bf16[512,256]{1,0:T(8,128)(2,1)} %copy-done.28) | copy-start | bytes 786436
  121.5 19.9 %collective-permute-start.18 = (bf16[384,1024]{1,0:T(8,128)(2,1)S(1)}, bf16[384,1024]{1,0:T(8,128)(2,1)S(1)}, u32[]{:S(2)}, u32[]{:S(2)}) collective-permute-start(bf16[384,1024]{1,0:T(8,128)(2,1)S(1)} %get-tuple-element.28), channel_id=1, source_target_pairs={{0,1},{1,0},{2,3},{3,2},{4,5},{5,4},{6,7},{7,6},{8,9},{9,8},{10,11... | collective-permute-start | bytes 2359304 | tf_op jit(solution)/shard_map/ppermute | solution.py:341
  135.1 14.5 %collective-permute-start.21 = (bf16[384,1024]{1,0:T(8,128)(2,1)}, bf16[384,1024]{1,0:T(8,128)(2,1)}, u32[]{:S(2)}, u32[]{:S(2)}) collective-permute-start(bf16[384,1024]{1,0:T(8,128)(2,1)} %get-tuple-element.32), channel_id=1, source_target_pairs={{0,1},{1,0},{2,3},{3,2},{4,5},{5,4},{6,7},{7,6},{8,9},{9,8},{10,11... | collective-permute-start | bytes 2359304 | tf_op jit(solution)/shard_map/ppermute | solution.py:341
  141.4 11.5 %collective-permute-start.15 = (bf16[384,1024]{1,0:T(8,128)(2,1)}, bf16[384,1024]{1,0:T(8,128)(2,1)S(1)}, u32[]{:S(2)}, u32[]{:S(2)}) collective-permute-start(bf16[384,1024]{1,0:T(8,128)(2,1)} %get-tuple-element.26), channel_id=1, source_target_pairs={{0,1},{1,0},{2,3},{3,2},{4,5},{5,4},{6,7},{7,6},{8,9},{9,8},{10,11... | collective-permute-start | bytes 2359304 | tf_op jit(solution)/shard_map/ppermute | solution.py:341
  142.5 20.7 %collective-permute-start.19 = (bf16[384,1024]{1,0:T(8,128)(2,1)}, bf16[384,1024]{1,0:T(8,128)(2,1)}, u32[]{:S(2)}, u32[]{:S(2)}) collective-permute-start(bf16[384,1024]{1,0:T(8,128)(2,1)} %shard_map.167), channel_id=1, source_target_pairs={{0,16},{16,0},{1,17},{17,1},{2,18},{18,2},{3,19},{19,3},{4,20},{20... | collective-permute-start | bytes 2359304 | tf_op jit(solution)/shard_map/ppermute | solution.py:338
  146.4 38.7 %collective-permute-start.20 = (bf16[384,1024]{1,0:T(8,128)(2,1)}, bf16[384,1024]{1,0:T(8,128)(2,1)}, u32[]{:S(2)}, u32[]{:S(2)}) collective-permute-start(bf16[384,1024]{1,0:T(8,128)(2,1)} %copy-done.17), channel_id=1, source_target_pairs={{0,1},{1,0},{2,3},{3,2},{4,5},{5,4},{6,7},{7,6},{8,9},{9,8},{10,11... | collective-permute-start | bytes 2359304 | tf_op jit(solution)/shard_map/ppermute | solution.py:341
  149.6 13.7 %copy-start.7 = (bf16[384,1024]{1,0:T(8,128)(2,1)S(1)}, bf16[384,1024]{1,0:T(8,128)(2,1)}, u32[]{:S(2)}) copy-start(bf16[384,1024]{1,0:T(8,128)(2,1)} %copy-done.6) | copy-start | bytes 2359300
  149.6 35.0 %collective-permute-start.25 = (bf16[256,1408]{1,0:T(8,128)(2,1)}, bf16[256,1408]{1,0:T(8,128)(2,1)}, u32[]{:S(2)}, u32[]{:S(2)}) collective-permute-start(bf16[256,1408]{1,0:T(8,128)(2,1)} %concatenate.21.rest_4_.rest_2_.rest_3_), channel_id=1, source_target_pairs={{0,4},{2,6},{4,12},{6,14},{12,8},{14,10},{8,0},{10,2},{1,5},{3,7},... | collective-permute-start | bytes 2162696 | tf_op jit(solution)/shard_map/ppermute | solution.py:346
  150.8 12.5 %copy-start.12 = (bf16[256,1408]{1,0:T(8,128)(2,1)S(1)}, bf16[256,1408]{1,0:T(8,128)(2,1)}, u32[]{:S(2)}) copy-start(bf16[256,1408]{1,0:T(8,128)(2,1)} %concatenate.21.rest_4_.rest_2_.rest_3_) | copy-start | bytes 2162692
  152.2 32.8 %collective-permute-start.22 = (bf16[384,1024]{1,0:T(8,128)(2,1)S(1)}, bf16[384,1024]{1,0:T(8,128)(2,1)S(1)}, u32[]{:S(2)}, u32[]{:S(2)}) collective-permute-start(bf16[384,1024]{1,0:T(8,128)(2,1)S(1)} %shard_map.169), channel_id=1, source_target_pairs={{0,16},{16,0},{1,17},{17,1},{2,18},{18,2},{3,19},{19,3},{4,20},{20... | collective-permute-start | bytes 2359304 | tf_op jit(solution)/shard_map/ppermute | solution.py:338
  153.8 12.3 %collective-permute-start.32 = (bf16[704,256]{1,0:T(8,128)(2,1)S(1)}, bf16[704,256]{1,0:T(8,128)(2,1)S(1)}, u32[]{:S(2)}, u32[]{:S(2)}) collective-permute-start(bf16[704,256]{1,0:T(8,128)(2,1)S(1)} %constant_dynamic-slice_fusion.4), channel_id=1, source_target_pairs={{0,2},{2,0},{4,6},{6,4},{8,10},{10,8},{12,14},{14,12},{1,3},{3,1},... | collective-permute-start | bytes 1081352 | tf_op jit(solution)/shard_map/ppermute | solution.py:356
  163.3 23.6 %collective-permute-start.27 = (bf16[256,1408]{1,0:T(8,128)(2,1)S(1)}, bf16[256,1408]{1,0:T(8,128)(2,1)}, u32[]{:S(2)}, u32[]{:S(2)}) collective-permute-start(bf16[256,1408]{1,0:T(8,128)(2,1)S(1)} %copy-done.12), channel_id=1, source_target_pairs={{4,0},{6,2},{12,4},{14,6},{8,12},{10,14},{0,8},{2,10},{5,1},{7,3},... | collective-permute-start | bytes 2162696 | tf_op jit(solution)/shard_map/ppermute | solution.py:348
  166.0 19.1 %copy-start.5 = (bf16[384,1024]{1,0:T(8,128)(2,1)S(1)}, bf16[384,1024]{1,0:T(8,128)(2,1)}, u32[]{:S(2)}) copy-start(bf16[384,1024]{1,0:T(8,128)(2,1)} %copy-done.4) | copy-start | bytes 2359300
  166.1 40.5 %collective-permute-start.37 = (bf16[384,1024]{1,0:T(8,128)(2,1)S(1)}, bf16[384,1024]{1,0:T(8,128)(2,1)}, u32[]{:S(2)}, u32[]{:S(2)}) collective-permute-start(bf16[384,1024]{1,0:T(8,128)(2,1)S(1)} %shard_map.168.rest_0_), channel_id=1, source_target_pairs={{0,16},{16,0},{1,17},{17,1},{2,18},{18,2},{3,19},{19,3},{4,20},{20... | collective-permute-start | bytes 2359304 | tf_op jit(solution)/shard_map/ppermute | solution.py:338
  167.7 19.2 %copy-start.15 = (bf16[1408,256]{1,0:T(8,128)(2,1)}, bf16[1408,256]{1,0:T(8,128)(2,1)S(1)}, u32[]{:S(2)}) copy-start(bf16[1408,256]{1,0:T(8,128)(2,1)S(1)} %pad_maximum_fusion.rest_0_) | copy-start | bytes 2162692
  184.6 17.5 %collective-permute-start.28 = (bf16[256,1408]{1,0:T(8,128)(2,1)S(1)}, bf16[256,1408]{1,0:T(8,128)(2,1)S(1)}, u32[]{:S(2)}, u32[]{:S(2)}) collective-permute-start(bf16[256,1408]{1,0:T(8,128)(2,1)S(1)} %copy-done.12), channel_id=1, source_target_pairs={{0,2},{2,0},{4,6},{6,4},{8,10},{10,8},{12,14},{14,12},{1,3},{3,1},... | collective-permute-start | bytes 2162696 | tf_op jit(solution)/shard_map/ppermute | solution.py:353
  185.1 19.9 %collective-permute-start.33 = (bf16[1408,256]{1,0:T(8,128)(2,1)S(1)}, bf16[1408,256]{1,0:T(8,128)(2,1)S(1)}, u32[]{:S(2)}, u32[]{:S(2)}) collective-permute-start(bf16[1408,256]{1,0:T(8,128)(2,1)S(1)} %pad_maximum_fusion.rest_0_), channel_id=1, source_target_pairs={{0,4},{2,6},{4,12},{6,14},{12,8},{14,10},{8,0},{10,2},{1,5},{3,7},... | collective-permute-start | bytes 2162696 | tf_op jit(solution)/shard_map/ppermute | solution.py:346
  185.1 33.7 %collective-permute-start.26 = (bf16[256,1408]{1,0:T(8,128)(2,1)}, bf16[256,1408]{1,0:T(8,128)(2,1)}, u32[]{:S(2)}, u32[]{:S(2)}) collective-permute-start(bf16[256,1408]{1,0:T(8,128)(2,1)} %collective-permute-done.25.rest_5_.rest_3_.rest_4_), channel_id=1, source_target_pairs={{0,4},{2,6},{4,12},{6,14},{12,8},{14,10},{8,0},{10,2},{1,5},{3,7},... | collective-permute-start | bytes 2162696 | tf_op jit(solution)/shard_map/ppermute | solution.py:346
  185.2 35.1 %copy-start.32 = (f32[2048]{0:T(1024)S(1)}, f32[2048]{0:T(1024)}, u32[]{:S(2)}) copy-start(f32[2048]{0:T(1024)} %param.27) | copy-start | bytes 24580
  185.2 35.4 %copy-start.33 = (f32[3,1408]{1,0:T(4,128)S(1)}, f32[3,1408]{1,0:T(4,128)}, u32[]{:S(2)}) copy-start(f32[3,1408]{1,0:T(4,128)} %param.31) | copy-start | bytes 50692
  185.2 35.4 %copy-start.34 = (f32[3,1408]{1,0:T(4,128)S(1)}, f32[3,1408]{1,0:T(4,128)}, u32[]{:S(2)}) copy-start(f32[3,1408]{1,0:T(4,128)} %param.30) | copy-start | bytes 50692
  186.8 19.7 %copy-start.2 = (bf16[384,1024]{1,0:T(8,128)(2,1)}, bf16[384,1024]{1,0:T(8,128)(2,1)S(1)}, u32[]{:S(2)}) copy-start(bf16[384,1024]{1,0:T(8,128)(2,1)S(1)} %shard_map.170.rest_1_) | copy-start | bytes 2359300
  186.8 33.4 %collective-permute-start.42 = (bf16[384,1024]{1,0:T(8,128)(2,1)S(1)}, bf16[384,1024]{1,0:T(8,128)(2,1)}, u32[]{:S(2)}, u32[]{:S(2)}) collective-permute-start(bf16[384,1024]{1,0:T(8,128)(2,1)S(1)} %shard_map.170.rest_1_), channel_id=1, source_target_pairs={{0,16},{16,0},{1,17},{17,1},{2,18},{18,2},{3,19},{19,3},{4,20},{20... | collective-permute-start | bytes 2359304 | tf_op jit(solution)/shard_map/ppermute | solution.py:338
  202.9 19.2 %collective-permute-start.29 = (bf16[256,1408]{1,0:T(8,128)(2,1)}, bf16[256,1408]{1,0:T(8,128)(2,1)S(1)}, u32[]{:S(2)}, u32[]{:S(2)}) collective-permute-start(bf16[256,1408]{1,0:T(8,128)(2,1)} %collective-permute-done.25.rest_5_.rest_3_.rest_4_), channel_id=1, source_target_pairs={{0,2},{2,0},{4,6},{6,4},{8,10},{10,8},{12,14},{14,12},{1,3},{3,1},... | collective-permute-start | bytes 2162696 | tf_op jit(solution)/shard_map/ppermute | solution.py:353
  205.0 15.3 %copy-start.18 = (bf16[1408,256]{1,0:T(8,128)(2,1)}, bf16[1408,256]{1,0:T(8,128)(2,1)S(1)}, u32[]{:S(2)}) copy-start(bf16[1408,256]{1,0:T(8,128)(2,1)S(1)} %collective-permute-done.33.rest_1_) | copy-start | bytes 2162692
  205.0 32.7 %collective-permute-start.31 = (bf16[256,1408]{1,0:T(8,128)(2,1)}, bf16[256,1408]{1,0:T(8,128)(2,1)}, u32[]{:S(2)}, u32[]{:S(2)}) collective-permute-start(bf16[256,1408]{1,0:T(8,128)(2,1)} %collective-permute-done.27.rest_7_.rest_5_.rest_6_), channel_id=1, source_target_pairs={{0,2},{2,0},{4,6},{6,4},{8,10},{10,8},{12,14},{14,12},{1,3},{3,1},... | collective-permute-start | bytes 2162696 | tf_op jit(solution)/shard_map/ppermute | solution.py:353
  206.5 44.4 %collective-permute-start.38 = (bf16[384,1024]{1,0:T(8,128)(2,1)}, bf16[384,1024]{1,0:T(8,128)(2,1)S(1)}, u32[]{:S(2)}, u32[]{:S(2)}) collective-permute-start(bf16[384,1024]{1,0:T(8,128)(2,1)} %collective-permute-done.37.rest_0_), channel_id=1, source_target_pairs={{0,1},{1,0},{2,3},{3,2},{4,5},{5,4},{6,7},{7,6},{8,9},{9,8},{10,11... | collective-permute-start | bytes 2359304 | tf_op jit(solution)/shard_map/ppermute | solution.py:341
  218.7 32.1 %collective-permute-start.30 = (bf16[256,1408]{1,0:T(8,128)(2,1)}, bf16[256,1408]{1,0:T(8,128)(2,1)}, u32[]{:S(2)}, u32[]{:S(2)}) collective-permute-start(bf16[256,1408]{1,0:T(8,128)(2,1)} %collective-permute-done.26.rest_6_.rest_4_.rest_5_), channel_id=1, source_target_pairs={{0,2},{2,0},{4,6},{6,4},{8,10},{10,8},{12,14},{14,12},{1,3},{3,1},... | collective-permute-start | bytes 2162696 | tf_op jit(solution)/shard_map/ppermute | solution.py:353
  220.3 41.5 %collective-permute-start.43 = (bf16[384,1024]{1,0:T(8,128)(2,1)}, bf16[384,1024]{1,0:T(8,128)(2,1)}, u32[]{:S(2)}, u32[]{:S(2)}) collective-permute-start(bf16[384,1024]{1,0:T(8,128)(2,1)} %collective-permute-done.42.rest_1_), channel_id=1, source_target_pairs={{0,1},{1,0},{2,3},{3,2},{4,5},{5,4},{6,7},{7,6},{8,9},{9,8},{10,11... | collective-permute-start | bytes 2359304 | tf_op jit(solution)/shard_map/ppermute | solution.py:341
  223.0 46.7 %collective-permute-start.35 = (bf16[1408,256]{1,0:T(8,128)(2,1)}, bf16[1408,256]{1,0:T(8,128)(2,1)}, u32[]{:S(2)}, u32[]{:S(2)}) collective-permute-start(bf16[1408,256]{1,0:T(8,128)(2,1)} %copy-done.15), channel_id=1, source_target_pairs={{4,0},{6,2},{12,4},{14,6},{8,12},{10,14},{0,8},{2,10},{5,1},{7,3},... | collective-permute-start | bytes 2162696 | tf_op jit(solution)/shard_map/ppermute | solution.py:348
  237.7 32.0 %collective-permute-start.34 = (bf16[1408,256]{1,0:T(8,128)(2,1)}, bf16[1408,256]{1,0:T(8,128)(2,1)}, u32[]{:S(2)}, u32[]{:S(2)}) collective-permute-start(bf16[1408,256]{1,0:T(8,128)(2,1)} %copy-done.18), channel_id=1, source_target_pairs={{0,4},{2,6},{4,12},{6,14},{12,8},{14,10},{8,0},{10,2},{1,5},{3,7},... | collective-permute-start | bytes 2162696 | tf_op jit(solution)/shard_map/ppermute | solution.py:346
  250.9 27.0 %collective-permute-start.23 = (bf16[384,1024]{1,0:T(8,128)(2,1)S(1)}, bf16[384,1024]{1,0:T(8,128)(2,1)S(1)}, u32[]{:S(2)}, u32[]{:S(2)}) collective-permute-start(bf16[384,1024]{1,0:T(8,128)(2,1)S(1)} %shard_map.168.rest_0_), channel_id=1, source_target_pairs={{0,1},{1,0},{2,3},{3,2},{4,5},{5,4},{6,7},{7,6},{8,9},{9,8},{10,11... | collective-permute-start | bytes 2359304 | tf_op jit(solution)/shard_map/ppermute | solution.py:341
  250.9 27.0 %collective-permute-start.24 = (bf16[384,1024]{1,0:T(8,128)(2,1)}, bf16[384,1024]{1,0:T(8,128)(2,1)S(1)}, u32[]{:S(2)}, u32[]{:S(2)}) collective-permute-start(bf16[384,1024]{1,0:T(8,128)(2,1)} %copy-done.2), channel_id=1, source_target_pairs={{0,1},{1,0},{2,3},{3,2},{4,5},{5,4},{6,7},{7,6},{8,9},{9,8},{10,11... | collective-permute-start | bytes 2359304 | tf_op jit(solution)/shard_map/ppermute | solution.py:341
  273.4 21.1 %collective-permute-start.44 = (bf16[384,1024]{1,0:T(8,128)(2,1)S(1)}, bf16[384,1024]{1,0:T(8,128)(2,1)S(1)}, u32[]{:S(2)}, u32[]{:S(2)}) collective-permute-start(bf16[384,1024]{1,0:T(8,128)(2,1)S(1)} %get-tuple-element.44), channel_id=1, source_target_pairs={{0,1},{1,0},{2,3},{3,2},{4,5},{5,4},{6,7},{7,6},{8,9},{9,8},{10,11... | collective-permute-start | bytes 2359304 | tf_op jit(solution)/shard_map/ppermute | solution.py:341
  277.3 18.3 %collective-permute-start.39 = (bf16[384,1024]{1,0:T(8,128)(2,1)S(1)}, bf16[384,1024]{1,0:T(8,128)(2,1)S(1)}, u32[]{:S(2)}, u32[]{:S(2)}) collective-permute-start(bf16[384,1024]{1,0:T(8,128)(2,1)S(1)} %get-tuple-element.38), channel_id=1, source_target_pairs={{0,1},{1,0},{2,3},{3,2},{4,5},{5,4},{6,7},{7,6},{8,9},{9,8},{10,11... | collective-permute-start | bytes 2359304 | tf_op jit(solution)/shard_map/ppermute | solution.py:341
  294.4 3.0 collective-permute-start.41
  294.8 20.5 %collective-permute-start.45 = (bf16[384,1024]{1,0:T(8,128)(2,1)S(1)}, bf16[384,1024]{1,0:T(8,128)(2,1)S(1)}, u32[]{:S(2)}, u32[]{:S(2)}) collective-permute-start(bf16[384,1024]{1,0:T(8,128)(2,1)S(1)} %shard_map.178), channel_id=1, source_target_pairs={{0,16},{16,0},{1,17},{17,1},{2,18},{18,2},{3,19},{19,3},{4,20},{20... | collective-permute-start | bytes 2359304 | tf_op jit(solution)/shard_map/ppermute | solution.py:338
  295.4 20.5 %collective-permute-start.36 = (bf16[384,1024]{1,0:T(8,128)(2,1)S(1)}, bf16[384,1024]{1,0:T(8,128)(2,1)S(1)}, u32[]{:S(2)}, u32[]{:S(2)}) collective-permute-start(bf16[384,1024]{1,0:T(8,128)(2,1)S(1)} %get-tuple-element.35), channel_id=1, source_target_pairs={{0,1},{1,0},{2,3},{3,2},{4,5},{5,4},{6,7},{7,6},{8,9},{9,8},{10,11... | collective-permute-start | bytes 2359304 | tf_op jit(solution)/shard_map/ppermute | solution.py:341
  295.8 35.8 %collective-permute-start.40 = (bf16[384,1024]{1,0:T(8,128)(2,1)S(1)}, bf16[384,1024]{1,0:T(8,128)(2,1)S(1)}, u32[]{:S(2)}, u32[]{:S(2)}) collective-permute-start(bf16[384,1024]{1,0:T(8,128)(2,1)S(1)} %shard_map.175), channel_id=1, source_target_pairs={{0,16},{16,0},{1,17},{17,1},{2,18},{18,2},{3,19},{19,3},{4,20},{20... | collective-permute-start | bytes 2359304 | tf_op jit(solution)/shard_map/ppermute | solution.py:338
  (20 other events, 52.5 us)
where the time goes:
time: 334 us; the launch traced here: 333 us
  waiting for transfers between devices  203 us (61%)
  Pallas kernels  81 us (24%)
  starting transfers between devices  24.5 us (7%)
  local copies, waits for them, and re-layouts  21.8 us (7%)
    pallas_call x10, Pallas kernels, call(): pl.pallas_call(functools.partial(kernel, len(pieces)), out_shape=outs, in...  74.7 us
    ppermute x9, waiting for transfers between devices, around(): found[k] = lax.ppermute(found[k - 1], 'fs', ring_pairs)  71.5 us
    ppermute x12, waiting for transfers between devices, gather_z_first(): return found + [lax.ppermute(q, 'fs', swap_pairs) for q in found]  69.3 us
    ppermute x7, waiting for transfers between devices, across(): return lax.ppermute(value, 'rep', flip)  62 us
    unnamed x76, local copies, waits for them, and re-layouts  12.8 us
    ppermute x12, starting transfers between devices, gather_z_first(): return found + [lax.ppermute(q, 'fs', swap_pairs) for q in found]  10.3 us
    ppermute x7, starting transfers between devices, across(): return lax.ppermute(value, 'rep', flip)  7.97 us
  transfers between devices with their start and end apart: 46, of which 17 were waited for; matrix products, arithmetic and copies ran while one was open for 3% of the time, Pallas kernels for 24%

commit v1 on v0

--- a/solution.py
+++ b/solution.py
@@ -39,14 +39,14 @@
     return copies
 
 
-def fetch_blocks(order_ref, pieces, wbuf, sems):
+def fetch_blocks(order_ref, pieces, wbuf, sems, first=0):
     blocks = wbuf.shape[0]
     per = blocks // len(pieces)
     rows = pieces[0].shape[0] // per
     copies = []
     for k in range(blocks):
         source = pieces[k % len(pieces)].at[pl.ds(k // len(pieces) * rows, rows)]
-        copies.append(pltpu.make_async_copy(source, wbuf.at[order_ref[k], pl.ds(0, rows)], sems.at[k]))
+        copies.append(pltpu.make_async_copy(source, wbuf.at[order_ref[k], pl.ds(0, rows)], sems.at[first + k]))
     return copies
 
 
@@ -182,21 +182,33 @@
     lax.fori_loop(0, out_ref.shape[0] // TILE, step, 0, unroll=2)
 
 
-def ffn_kernel(halo, chunks, n_pieces, order_ref, gain_ref, taps_ref, *rest):
+def final_kernel(start, chained, *refs):
+    terms = refs[:4]
+    out_ref, buffer_ref, sem = refs[4 + chained :]
+    add_kernel([0] * 4, *terms, buffer_ref)
+    copy = pltpu.make_async_copy(buffer_ref, out_ref.at[pl.ds(start, buffer_ref.shape[0])], sem)
+    copy.start()
+    copy.wait()
+
+
+def ffn_kernel(halo, chunks, parts, n_down, n_pieces, order_ref, gain_ref, taps_ref, *rest):
     if halo:
         before_ref, rest = rest[0], rest[1:]
     n_streams = 2 * chunks
-    n_pieces -= n_streams
-    streams, pieces = rest[:n_streams], rest[n_streams : n_pieces + n_streams]
-    hidden_ref, after_ref, own_ref, peer_ref, normed_ref, wbuf, pre_ref, sems = rest[n_pieces + n_streams :]
+    streams, pieces, downs = rest[:n_streams], rest[n_streams : n_pieces - n_down], rest[n_pieces - n_down : n_pieces]
+    outs, after_ref = rest[n_pieces : n_pieces + 2 * parts], rest[n_pieces + 2 * parts]
+    own_ref, peer_ref, normed_ref, wbuf, pre_ref, hidden_ref, down_ref, sems = rest[n_pieces + 2 * parts + 1 :]
+    n_pieces -= n_streams + n_down
     buffers = []
     for k, stream in enumerate(streams):
         rows = stream.shape[0]
         buffers.append((own_ref, peer_ref)[k // chunks].at[pl.ds(k % chunks * rows, rows)])
     stream_copies = fetch_streams(streams, buffers, sems, n_pieces)
     copies = fetch_rows(order_ref, pieces, wbuf, sems)
-    for copy in stream_copies + copies:
+    down_copies = fetch_blocks(order_ref, downs, down_ref, sems, n_pieces + n_streams)
+    for copy in stream_copies + copies + down_copies:
         copy.start()
+    clear_padding(downs, down_ref)
     for copy in stream_copies:
         copy.wait()
     length = own_ref.shape[0]
@@ -242,24 +254,23 @@
 
     lax.fori_loop(0, length // rows, project, 0)
     after_ref[...] = pre_ref[0:8, :]
-
-
-def out_kernel(parts, n_pieces, order_ref, left_ref, *rest):
-    pieces = rest[:n_pieces]
-    keeps, sends = rest[n_pieces : n_pieces + parts], rest[n_pieces + parts : n_pieces + 2 * parts]
-    wbuf, sems = rest[n_pieces + 2 * parts :]
-    copies = fetch_blocks(order_ref, pieces, wbuf, sems)
-    for copy in copies:
-        copy.start()
+    for copy in down_copies:
+        copy.wait()
+    multiply_out(hidden_ref, down_ref, outs[:parts], outs[parts:])
+
+
+def clear_padding(pieces, wbuf):
     blocks, padded, width = wbuf.shape
     depth = pieces[0].shape[0] * len(pieces) // blocks
     if padded > depth:
         wbuf[:, depth:, :] = jnp.zeros((blocks, padded - depth, width), BF16)
+
+
+def multiply_out(left_ref, wbuf, keeps, sends):
+    blocks, _, width = wbuf.shape
     length = keeps[0].shape[0]
     rows = row_block(length)
-    for copy in copies:
-        copy.wait()
-    for part in range(parts):
+    for part in range(len(keeps)):
 
         def step(m, _):
             at = pl.multiple_of(m * rows, rows)
@@ -272,6 +283,19 @@
             return 0
 
         lax.fori_loop(0, length // rows, step, 0)
+
+
+def out_kernel(parts, n_pieces, order_ref, left_ref, *rest):
+    pieces = rest[:n_pieces]
+    keeps, sends = rest[n_pieces : n_pieces + parts], rest[n_pieces + parts : n_pieces + 2 * parts]
+    wbuf, sems = rest[n_pieces + 2 * parts :]
+    copies = fetch_blocks(order_ref, pieces, wbuf, sems)
+    for copy in copies:
+        copy.start()
+    clear_padding(pieces, wbuf)
+    for copy in copies:
+        copy.wait()
+    multiply_out(left_ref, wbuf, keeps, sends)
 
 
 def call(kernel, outs, scratch, limit_mib, flops, operands, pieces, copies=None):
@@ -340,7 +364,7 @@
     def partner(value):
         return lax.ppermute(value, "tp", flip)
 
-    def around(own, ahead=outer // 2):
+    def around(own, ahead=outer - 1):
         found = {0: own}
         for k in range(1, ahead + 1):
             found[k] = lax.ppermute(found[k - 1], "fs", ring_pairs)
@@ -348,7 +372,7 @@
             found[k] = lax.ppermute(found[(k + 1) % outer], "fs", back_pairs)
         return [found[k] for k in range(outer)]
 
-    def gather_z_first(own, ahead=outer // 2):
+    def gather_z_first(own, ahead=outer - 1):
         found = around(own, ahead)
         return found + [lax.ppermute(q, "fs", swap_pairs) for q in found]
 
@@ -376,12 +400,13 @@
         return jnp.concatenate([gate[:, :full], up[:, :full], gate[:, full:], up[:, full:]], axis=1)
 
     both = jnp.concatenate([half_of(lin_weight, 1), half_of(branch_weight, 1)], axis=1)
-    mix_pieces = gather_z_first(both, outer - 1)
+    mix_pieces = gather_z_first(both)
     other = across(own)
     own_peer = partner(own)
     other_peer = partner(other)
     out_pieces = gather_z_first(half_of(out_weight, 0))
-    ffn_pieces = gather_z_first(interleave(gate_weight, up_weight))
+    both = interleave(gate_weight, up_weight)
+    ffn_pieces = gather_z_first(both)
     down_pieces = gather_y_first(half_of(down_weight, 0))
 
     gates = jnp.concatenate([half_of(rate_blocks, 0), half_of(admit_blocks, 0)], axis=2)
@@ -431,23 +456,30 @@
 
     def ffn(owns, peers, before):
         width = 2 * units
-        rows = len(owns) * part
+        parts = len(owns)
+        rows = parts * part
         halo = [] if before is None else [before]
-        return call(
-            functools.partial(ffn_kernel, bool(halo), len(owns)),
-            (jax.ShapeDtypeStruct((rows, padded_units), BF16), jax.ShapeDtypeStruct((8, width), F32)),
+        pieces = owns + peers + ffn_pieces + down_pieces
+        sums = [jax.ShapeDtypeStruct((part, half), BF16)] * (2 * parts)
+        outs = call(
+            functools.partial(ffn_kernel, bool(halo), parts, parts, len(down_pieces)),
+            sums + [jax.ShapeDtypeStruct((8, width), F32)],
             [
                 pltpu.VMEM((rows, half), BF16),
                 pltpu.VMEM((rows, half), BF16),
                 pltpu.VMEM((rows, 2 * half), BF16),
                 pltpu.VMEM((2 * half, width), BF16),
                 pltpu.VMEM((row_block(rows) + 8, width), F32),
+                pltpu.VMEM((rows, padded_units), BF16),
+                pltpu.VMEM((n_fs, padded_units, down_pieces[0].shape[1]), BF16),
             ],
-            28,
-            rows * 2 * half * width * 2,
+            36,
+            rows * 2 * half * width * 3,
             [order, gain2, ffn_taps] + halo,
-            owns + peers + ffn_pieces,
+            pieces,
+            len(pieces) + n_fs,
         )
+        return outs[:parts], outs[parts : 2 * parts], outs[2 * parts]
 
     def add(*terms):
         starts = [t[1] if isinstance(t, tuple) else 0 for t in terms]
@@ -479,16 +511,24 @@
 
     tail, sent = None, []
     for i in range(PARTS):
-        hidden, tail = ffn([middle_other[i]], [other_middle_peer[i]], tail)
-        keep, send = project(hidden, down_pieces)
+        keep, send, tail = ffn([middle_other[i]], [other_middle_peer[i]], tail)
         sent.append(across(add(keep[0], partner(send[0]))))
-    hidden, _ = ffn(middle, middle_peer, None)
-    keeps, sends = project(hidden, down_pieces)
+    keeps, sends, _ = ffn(middle, middle_peer, None)
     result = []
     for i in range(PARTS):
         terms = [middle[i], keeps[i], partner(sends[i]), sent[i]]
-        result.append(functools.reduce(jnp.add, [t.astype(F32) for t in terms]).astype(BF16))
-    return jnp.concatenate(result, axis=0)[None]
+        run = pl.pallas_call(
+            functools.partial(final_kernel, i * part, len(result)),
+            out_shape=jax.ShapeDtypeStruct((length, half), BF16),
+            in_specs=[VMEM] * 4 + [HBM] * len(result),
+            out_specs=HBM,
+            scratch_shapes=[pltpu.VMEM((part, half), BF16), pltpu.SemaphoreType.DMA],
+            input_output_aliases={4: 0} if result else {},
+            compiler_params=pltpu.CompilerParams(vmem_limit_bytes=12 * 1024 * 1024),
+            cost_estimate=pl.CostEstimate(flops=part * half * 4, bytes_accessed=2**21, transcendentals=0),
+        )
+        result = [run(*terms, *result)]
+    return result[0][None]
 
 
 def solution(mesh):

time: 334 us -> 330 us (0.988)
  the two profiles are of different devices: /device:TPU:28 before, /device:TPU:0 now
where the time goes in v1:
time: 330 us; the launch traced here: 329 us
  waiting for transfers between devices  182 us (55%)
  Pallas kernels  73.8 us (22%)
  starting transfers between devices  44.2 us (13%)
  local copies, waits for them, and re-layouts  27.1 us (8%)
    ppermute x12, waiting for transfers between devices, around(): found[k] = lax.ppermute(found[k - 1], 'fs', ring_pairs)  82.5 us
    pallas_call x7, Pallas kernels, call(): pl.pallas_call(functools.partial(kernel, len(pieces)), out_shape=outs, in...  68 us
    ppermute x7, waiting for transfers between devices, across(): return lax.ppermute(value, 'rep', flip)  66.6 us
    ppermute x12, waiting for transfers between devices, gather_z_first(): return found + [lax.ppermute(q, 'fs', swap_pairs) for q in found]  27 us
    unnamed x108, local copies, waits for them, and re-layouts  17.4 us
    ppermute x12, starting transfers between devices, around(): found[k] = lax.ppermute(found[k - 1], 'fs', ring_pairs)  15.2 us
    ppermute x12, starting transfers between devices, gather_z_first(): return found + [lax.ppermute(q, 'fs', swap_pairs) for q in found]  14 us
    ppermute x7, starting transfers between devices, across(): return lax.ppermute(value, 'rep', flip)  11.3 us
  transfers between devices with their start and end apart: 46, of which 22 were waited for; matrix products, arithmetic and copies ran while one was open for 3% of the time, Pallas kernels for 22%

profile of v1, /device:TPU:0, one launch (start us, length us, event | category | flops | bytes accessed | tf_op | source)
XLA Modules:
  0.0 329.2 jit_solution(10623983368021963030)
XLA Ops:
  0.0 3.0 collective-permute-start.16
  3.1 1.1 constant_dynamic-slice_fusion.10
  4.3 1.6 collective-permute-start.1
  5.9 12.8 %collective-permute-done.1.rest_3_ = bf16[256,1024]{1,0:T(8,128)(2,1)} collective-permute-done((bf16[256,1024]{1,0:T(8,128)(2,1)S(1)}, bf16[256,1024]{1,0:T(8,128)(2,1)}, u32[]{:S(2)}, u32[]{:S(2)}) %collective-permute-start.1) | collective-permute-done | bytes 524320 | tf_op jit(solution)/shard_map/ppermute | solution.py:370
  19.4 18.4 %collective-permute-done.16.rest_0_ = bf16[768,1024]{1,0:T(8,128)(2,1)} collective-permute-done((bf16[768,1024]{1,0:T(8,128)(2,1)}, bf16[768,1024]{1,0:T(8,128)(2,1)}, u32[]{:S(2)}, u32[]{:S(2)}) %collective-permute-start.16) | collective-permute-done | bytes 1572896 | tf_op jit(solution)/shard_map/ppermute | solution.py:362
  37.8 1.9 collective-permute-start.8
  39.7 8.0 %collective-permute-done.8.rest_1_ = bf16[512,256]{1,0:T(8,128)(2,1)S(1)} collective-permute-done((bf16[512,256]{1,0:T(8,128)(2,1)S(1)}, bf16[512,256]{1,0:T(8,128)(2,1)S(1)}, u32[]{:S(2)}, u32[]{:S(2)}) %collective-permute-start.8) | collective-permute-done | bytes 262176 | tf_op jit(solution)/shard_map/ppermute | solution.py:370
  48.5 1.5 collective-permute-start.4
  50.0 3.4 %collective-permute-start.3 = (bf16[256,1024]{1,0:T(8,128)(2,1)}, bf16[256,1024]{1,0:T(8,128)(2,1)}, u32[]{:S(2)}, u32[]{:S(2)}) collective-permute-start(bf16[256,1024]{1,0:T(8,128)(2,1)} %collective-permute-done.2.rest_4_), channel_id=1, source_target_pairs={{0,4},{2,6},{4,12},{6,14},{12,8},{14,10},{8,0},{10,2},{1,5},{3,7},... | collective-permute-start | bytes 1572872 | tf_op jit(solution)/shard_map/ppermute | solution.py:370
  53.4 4.4 %collective-permute-done.9.rest_2_ = bf16[512,256]{1,0:T(8,128)(2,1)} collective-permute-done((bf16[512,256]{1,0:T(8,128)(2,1)S(1)}, bf16[512,256]{1,0:T(8,128)(2,1)}, u32[]{:S(2)}, u32[]{:S(2)}) %collective-permute-start.9) | collective-permute-done | bytes 262176 | tf_op jit(solution)/shard_map/ppermute | solution.py:370
  58.7 1.6 constant_dynamic-slice_fusion.12
  60.3 1.5 collective-permute-done.4.rest_6_
  61.8 1.5 collective-permute-start.5
  63.3 10.3 %collective-permute-done.10.rest_3_ = bf16[512,256]{1,0:T(8,128)(2,1)} collective-permute-done((bf16[512,256]{1,0:T(8,128)(2,1)}, bf16[512,256]{1,0:T(8,128)(2,1)}, u32[]{:S(2)}, u32[]{:S(2)}) %collective-permute-start.10) | collective-permute-done | bytes 262176 | tf_op jit(solution)/shard_map/ppermute | solution.py:370
  73.6 1.4 collective-permute-start.6
  77.6 2.4 constant_dynamic-slice_fusion
  80.0 1.4 collective-permute-start.11
  81.4 7.2 %collective-permute-done.6.rest_8_ = bf16[256,1024]{1,0:T(8,128)(2,1)} collective-permute-done((bf16[256,1024]{1,0:T(8,128)(2,1)}, bf16[256,1024]{1,0:T(8,128)(2,1)}, u32[]{:S(2)}, u32[]{:S(2)}) %collective-permute-start.6) | collective-permute-done | bytes 524320 | tf_op jit(solution)/shard_map/ppermute | solution.py:377
  88.7 1.4 collective-permute-start.12
  90.1 9.9 %collective-permute-done.7.rest_9_ = bf16[256,1024]{1,0:T(8,128)(2,1)} collective-permute-done((bf16[256,1024]{1,0:T(8,128)(2,1)}, bf16[256,1024]{1,0:T(8,128)(2,1)}, u32[]{:S(2)}, u32[]{:S(2)}) %collective-permute-start.7) | collective-permute-done | bytes 524320 | tf_op jit(solution)/shard_map/ppermute | solution.py:377
  99.9 1.4 collective-permute-start.13
  102.0 14.0 %shard_map.165.left_ref = bf16[768,512]{1,0:T(8,128)(2,1)S(1)} custom-call(s32[8]{0:T(128)S(1)} %fusion.1.order_ref, f32[2,1024]{1,0:T(2,128)S(1)} %broadcast_select_fusion.1.gain_ref, f32[4,512]{1,0:T(4,128)S(1)} %constant_dynamic-slice_fusion.14.taps_ref, bf16[4,128,256]{2,1,0:T(8,128)(2,1)S(1)} %pad_maximum_fusion.2.gates_ref, f32[1,512]{1,0:T(1,128)S(1)} %bitcast.11, ...), custom_call_target="tpu_custom_call" | custom-call | flops 3221225472 | bytes 4194304 | tf_op jit(solution)/shard_map/pallas_call | solution.py:303
  116.7 3.6 %collective-permute-done.14.rest_7_ = bf16[512,256]{1,0:T(8,128)(2,1)S(1)} collective-permute-done((bf16[512,256]{1,0:T(8,128)(2,1)}, bf16[512,256]{1,0:T(8,128)(2,1)S(1)}, u32[]{:S(2)}, u32[]{:S(2)}) %collective-permute-start.14) | collective-permute-done | bytes 262176 | tf_op jit(solution)/shard_map/ppermute | solution.py:377
  121.3 4.0 %shard_map.166 = (bf16[384,1024]{1,0:T(8,128)(2,1)S(1)}, bf16[384,1024]{1,0:T(8,128)(2,1)S(1)}, bf16[384,1024]{1,0:T(8,128)(2,1)}, bf16[384,1024]{1,0:T(8,128)(2,1)S(1)}) custom-call(s32[8]{0:T(128)S(1)} %fusion.1.order_ref, bf16[768,512]{1,0:T(8,128)(2,1)S(1)} %shard_map.165.left_ref, bf16[512,256]{1,0:T(8,128)(2,1)S(1)} %constant_dynamic-slice_fusion.9.rest_0_, ...), custom_call_target="tpu_custom_call" | custom-call | flops 1610612736 | bytes 4194304 | tf_op jit(solution)/shard_map/pallas_call | solution.py:303
  128.1 2.0 concatenate.18.rest_4_.rest_2_.rest_3_
  130.1 2.4 collective-permute-start.25
  132.4 1.0 copy-done.13
  134.4 13.6 %shard_map.163.left_ref = bf16[768,512]{1,0:T(8,128)(2,1)S(1)} custom-call(s32[8]{0:T(128)S(1)} %fusion.1.order_ref, f32[2,1024]{1,0:T(2,128)S(1)} %broadcast_select_fusion.1.gain_ref, f32[4,512]{1,0:T(4,128)S(1)} %constant_dynamic-slice_fusion.14.taps_ref, bf16[4,128,256]{2,1,0:T(8,128)(2,1)S(1)} %copy-done.15, f32[1,512]{1,0:T(1,128)S(1)} %bitcast.12, ...), custom_call_target="tpu_custom_call" | custom-call | flops 3221225472 | bytes 4194304 | tf_op jit(solution)/shard_map/pallas_call | solution.py:303
  148.1 3.5 %shard_map.164 = (bf16[384,1024]{1,0:T(8,128)(2,1)S(1)}, bf16[384,1024]{1,0:T(8,128)(2,1)S(1)}, bf16[384,1024]{1,0:T(8,128)(2,1)S(1)}, bf16[384,1024]{1,0:T(8,128)(2,1)S(1)}) custom-call(s32[8]{0:T(128)S(1)} %fusion.1.order_ref, bf16[768,512]{1,0:T(8,128)(2,1)S(1)} %shard_map.163.left_ref, bf16[512,256]{1,0:T(8,128)(2,1)S(1)} %constant_dynamic-slice_fusion.9.rest_0_, ...), custom_call_target="tpu_custom_call" | custom-call | flops 1610612736 | bytes 4194304 | tf_op jit(solution)/shard_map/pallas_call | solution.py:303
  152.2 1.6 collective-permute-start.32
  153.8 1.4 shard_map.169
  155.2 1.6 collective-permute-start.22
  156.8 6.1 %collective-permute-done.32 = bf16[704,256]{1,0:T(8,128)(2,1)S(1)} collective-permute-done((bf16[704,256]{1,0:T(8,128)(2,1)S(1)}, bf16[704,256]{1,0:T(8,128)(2,1)S(1)}, u32[]{:S(2)}, u32[]{:S(2)}) %collective-permute-start.32) | collective-permute-done | bytes 360480 | tf_op jit(solution)/shard_map/ppermute | solution.py:380
  162.9 1.5 collective-permute-start.33
  164.7 1.6 collective-permute-start.19
  166.5 9.2 %collective-permute-done.22.refs_3_ = bf16[384,1024]{1,0:T(8,128)(2,1)S(1)} collective-permute-done((bf16[384,1024]{1,0:T(8,128)(2,1)S(1)}, bf16[384,1024]{1,0:T(8,128)(2,1)S(1)}, u32[]{:S(2)}, u32[]{:S(2)}) %collective-permute-start.22) | collective-permute-done | bytes 786464 | tf_op jit(solution)/shard_map/ppermute | solution.py:362
  176.7 6.2 %collective-permute-done.33.rest_13_.rest_11_.rest_12_ = bf16[1408,256]{1,0:T(8,128)(2,1)S(1)} collective-permute-done((bf16[1408,256]{1,0:T(8,128)(2,1)S(1)}, bf16[1408,256]{1,0:T(8,128)(2,1)S(1)}, u32[]{:S(2)}, u32[]{:S(2)}) %collective-permute-start.33) | collective-permute-done | bytes 720928 | tf_op jit(solution)/shard_map/ppermute | solution.py:370
  182.9 1.5 collective-permute-start.37
  184.3 12.5 %collective-permute-done.26.rest_6_.rest_4_.rest_5_ = bf16[256,1408]{1,0:T(8,128)(2,1)} collective-permute-done((bf16[256,1408]{1,0:T(8,128)(2,1)S(1)}, bf16[256,1408]{1,0:T(8,128)(2,1)}, u32[]{:S(2)}, u32[]{:S(2)}) %collective-permute-start.26) | collective-permute-done | bytes 720928 | tf_op jit(solution)/shard_map/ppermute | solution.py:370
  196.8 1.5 collective-permute-start.29
  198.9 1.4 collective-permute-start.27
  201.8 1.5 collective-permute-start.39
  203.2 6.2 %collective-permute-done.37.rest_0_ = bf16[384,1024]{1,0:T(8,128)(2,1)} collective-permute-done((bf16[384,1024]{1,0:T(8,128)(2,1)S(1)}, bf16[384,1024]{1,0:T(8,128)(2,1)}, u32[]{:S(2)}, u32[]{:S(2)}) %collective-permute-start.37) | collective-permute-done | bytes 786464 | tf_op jit(solution)/shard_map/ppermute | solution.py:362
  209.5 3.9 %collective-permute-done.29.rest_9_.rest_7_.rest_8_ = bf16[256,1408]{1,0:T(8,128)(2,1)S(1)} collective-permute-done((bf16[256,1408]{1,0:T(8,128)(2,1)S(1)}, bf16[256,1408]{1,0:T(8,128)(2,1)S(1)}, u32[]{:S(2)}, u32[]{:S(2)}) %collective-permute-start.29) | collective-permute-done | bytes 720928 | tf_op jit(solution)/shard_map/ppermute | solution.py:377
  214.3 1.5 collective-permute-start.30
  215.8 2.6 collective-permute-done.34.rest_14_.rest_12_.rest_13_
  218.4 15.4 %collective-permute-done.27.rest_7_.rest_5_.rest_6_ = bf16[256,1408]{1,0:T(8,128)(2,1)} collective-permute-done((bf16[256,1408]{1,0:T(8,128)(2,1)}, bf16[256,1408]{1,0:T(8,128)(2,1)}, u32[]{:S(2)}, u32[]{:S(2)}) %collective-permute-start.27) | collective-permute-done | bytes 720928 | tf_op jit(solution)/shard_map/ppermute | solution.py:370
  236.1 10.4 %collective-permute-done.35.rest_15_.rest_13_.rest_14_ = bf16[1408,256]{1,0:T(8,128)(2,1)} collective-permute-done((bf16[1408,256]{1,0:T(8,128)(2,1)}, bf16[1408,256]{1,0:T(8,128)(2,1)}, u32[]{:S(2)}, u32[]{:S(2)}) %collective-permute-start.35) | collective-permute-done | bytes 720928 | tf_op jit(solution)/shard_map/ppermute | solution.py:370
  247.7 1.1 copy-done.7
  248.8 1.1 copy-done.10
  249.9 1.1 copy-done.19
  251.1 1.1 copy-done.21
  252.2 1.1 copy-done.24
  253.3 1.1 copy-done.27
  254.4 1.1 copy-done.30
  255.5 1.1 copy-done.33
  256.7 9.0 %shard_map.172 = (bf16[384,1024]{1,0:T(8,128)(2,1)S(1)}, bf16[384,1024]{1,0:T(8,128)(2,1)S(1)}, f32[8,1408]{1,0:T(8,128)S(1)}) custom-call(s32[8]{0:T(128)S(1)} %fusion.1.order_ref, f32[2,1024]{1,0:T(2,128)S(1)} %broadcast_select_fusion.gain_ref, f32[3,1408]{1,0:T(4,128)S(1)} %concatenate.17.taps_ref, bf16[384,1024]{1,0:T(8,128)(2,1)} %collective-permute-done.37.rest_0_, ...), custom_call_target="tpu_custom_call" | custom-call | flops 3321888768 | bytes 4194304 | tf_op jit(solution)/shard_map/pallas_call | solution.py:303
  266.1 9.0 %shard_map.173 = (bf16[384,1024]{1,0:T(8,128)(2,1)S(1)}, bf16[384,1024]{1,0:T(8,128)(2,1)S(1)}, f32[8,1408]{1,0:T(8,128)}) custom-call(s32[8]{0:T(128)S(1)} %fusion.1.order_ref, f32[2,1024]{1,0:T(2,128)S(1)} %broadcast_select_fusion.gain_ref, f32[3,1408]{1,0:T(4,128)S(1)} %concatenate.17.taps_ref, f32[8,1408]{1,0:T(8,128)S(1)} %get-tuple-element.32.rest_0_, ...), custom_call_target="tpu_custom_call" | custom-call | flops 3321888768 | bytes 4194304 | tf_op jit(solution)/shard_map/pallas_call | solution.py:303
  275.4 15.0 %shard_map.171 = (bf16[384,1024]{1,0:T(8,128)(2,1)S(1)}, bf16[384,1024]{1,0:T(8,128)(2,1)S(1)}, bf16[384,1024]{1,0:T(8,128)(2,1)S(1)}, bf16[384,1024]{1,0:T(8,128)(2,1)S(1)}, f32[8,1408]{1,0:T(8,128)}) custom-call(s32[8]{0:T(128)S(1)} %fusion.1.order_ref, f32[2,1024]{1,0:T(2,128)S(1)} %broadcast_select_fusion.gain_ref, f32[3,1408]{1,0:T(4,128)S(1)} %concatenate.17.taps_ref, ...), custom_call_target="tpu_custom_call" | custom-call | flops 6643777536 | bytes 4194304 | tf_op jit(solution)/shard_map/pallas_call | solution.py:303
  291.1 1.6 collective-permute-start.45
  293.5 18.1 %collective-permute-done.45.refs_3_ = bf16[384,1024]{1,0:T(8,128)(2,1)S(1)} collective-permute-done((bf16[384,1024]{1,0:T(8,128)(2,1)S(1)}, bf16[384,1024]{1,0:T(8,128)(2,1)S(1)}, u32[]{:S(2)}, u32[]{:S(2)}) %collective-permute-start.45) | collective-permute-done | bytes 786464 | tf_op jit(solution)/shard_map/ppermute | solution.py:362
  311.6 1.3 shard_map.176.refs_4_
  312.9 14.7 %collective-permute-done.42.refs_3_ = bf16[384,1024]{1,0:T(8,128)(2,1)S(1)} collective-permute-done((bf16[384,1024]{1,0:T(8,128)(2,1)S(1)}, bf16[384,1024]{1,0:T(8,128)(2,1)S(1)}, u32[]{:S(2)}, u32[]{:S(2)}) %collective-permute-start.42) | collective-permute-done | bytes 786464 | tf_op jit(solution)/shard_map/ppermute | solution.py:362
  327.6 1.4 shard_map.177
  (174 shorter events, 21.9 us)
Async XLA Ops:
  0.0 152.2 %copy-start = (bf16[1408,256]{1,0:T(8,128)(2,1)S(1)}, bf16[1408,256]{1,0:T(8,128)(2,1)}, u32[]{:S(2)}) copy-start(bf16[1408,256]{1,0:T(8,128)(2,1)} %param.32) | copy-start | bytes 2162692
  0.0 53.4 %copy-start.1 = (bf16[1,768,1024]{2,1,0:T(8,128)(2,1)S(1)}, bf16[1,768,1024]{2,1,0:T(8,128)(2,1)}, u32[]{:S(2)}) copy-start(bf16[1,768,1024]{2,1,0:T(8,128)(2,1)} %param.17) | copy-start | bytes 4718596
  0.0 58.6 %copy-start.52 = (f32[1024]{0:T(1024)S(1)}, f32[1024]{0:T(1024)}, u32[]{:S(2)}) copy-start(f32[1024]{0:T(1024)} %param.24) | copy-start | bytes 12292
  0.0 58.7 %copy-start.51 = (f32[4,1024]{1,0:T(4,128)S(1)}, f32[4,1024]{1,0:T(4,128)}, u32[]{:S(2)}) copy-start(f32[4,1024]{1,0:T(4,128)} %param.21) | copy-start | bytes 49156
  0.0 37.8 %collective-permute-start.16 = (bf16[768,1024]{1,0:T(8,128)(2,1)}, bf16[768,1024]{1,0:T(8,128)(2,1)}, u32[]{:S(2)}, u32[]{:S(2)}) collective-permute-start(bf16[768,1024]{1,0:T(8,128)(2,1)} %bitcast.6), channel_id=1, source_target_pairs={{0,16},{16,0},{1,17},{17,1},{2,18},{18,2},{3,19},{19,3},{4,20},{20... | collective-permute-start | bytes 4718600 | tf_op jit(solution)/shard_map/ppermute | solution.py:362
  3.1 34.7 %copy-start.46 = (bf16[1024,256]{1,0:T(8,128)(2,1)S(1)}, bf16[1024,256]{1,0:T(8,128)(2,1)}, u32[]{:S(2)}) copy-start(bf16[1024,256]{1,0:T(8,128)(2,1)} %param.26) | copy-start | bytes 1572868
  3.1 73.2 %copy-start.53 = (f32[1024]{0:T(1024)S(1)}, f32[1024]{0:T(1024)}, u32[]{:S(2)}) copy-start(f32[1024]{0:T(1024)} %param.25) | copy-start | bytes 12292
  3.1 73.3 %copy-start.47 = (f32[2048]{0:T(1024)S(1)}, f32[2048]{0:T(1024)}, u32[]{:S(2)}) copy-start(f32[2048]{0:T(1024)} %param.18) | copy-start | bytes 24580
  4.2 111.7 %copy-start.12 = (bf16[256,1024]{1,0:T(8,128)(2,1)}, bf16[256,1024]{1,0:T(8,128)(2,1)S(1)}, u32[]{:S(2)}) copy-start(bf16[256,1024]{1,0:T(8,128)(2,1)S(1)} %pad_maximum_fusion.1.rest_2_) | copy-start | bytes 1572868
  4.3 14.4 %collective-permute-start.1 = (bf16[256,1024]{1,0:T(8,128)(2,1)S(1)}, bf16[256,1024]{1,0:T(8,128)(2,1)}, u32[]{:S(2)}, u32[]{:S(2)}) collective-permute-start(bf16[256,1024]{1,0:T(8,128)(2,1)S(1)} %pad_maximum_fusion.1.rest_2_), channel_id=1, source_target_pairs={{0,4},{2,6},{4,12},{6,14},{12,8},{14,10},{8,0},{10,2},{1,5},{3,7},... | collective-permute-start | bytes 1572872 | tf_op jit(solution)/shard_map/ppermute | solution.py:370
  18.7 31.3 %collective-permute-start.2 = (bf16[256,1024]{1,0:T(8,128)(2,1)}, bf16[256,1024]{1,0:T(8,128)(2,1)}, u32[]{:S(2)}, u32[]{:S(2)}) collective-permute-start(bf16[256,1024]{1,0:T(8,128)(2,1)} %collective-permute-done.1.rest_3_), channel_id=1, source_target_pairs={{0,4},{2,6},{4,12},{6,14},{12,8},{14,10},{8,0},{10,2},{1,5},{3,7},... | collective-permute-start | bytes 1572872 | tf_op jit(solution)/shard_map/ppermute | solution.py:370
  37.8 63.5 %collective-permute-start.17 = (bf16[768,1024]{1,0:T(8,128)(2,1)}, bf16[768,1024]{1,0:T(8,128)(2,1)}, u32[]{:S(2)}, u32[]{:S(2)}) collective-permute-start(bf16[768,1024]{1,0:T(8,128)(2,1)} %collective-permute-done.16.rest_0_), channel_id=1, source_target_pairs={{0,1},{1,0},{2,3},{3,2},{4,5},{5,4},{6,7},{7,6},{8,9},{9,8},{10,11... | collective-permute-start | bytes 4718600 | tf_op jit(solution)/shard_map/ppermute | solution.py:365
  37.8 9.9 %collective-permute-start.8 = (bf16[512,256]{1,0:T(8,128)(2,1)S(1)}, bf16[512,256]{1,0:T(8,128)(2,1)S(1)}, u32[]{:S(2)}, u32[]{:S(2)}) collective-permute-start(bf16[512,256]{1,0:T(8,128)(2,1)S(1)} %constant_dynamic-slice_fusion.9.rest_0_), channel_id=1, source_target_pairs={{0,4},{2,6},{4,12},{6,14},{12,8},{14,10},{8,0},{10,2},{1,5},{3,7},... | collective-permute-start | bytes 786440 | tf_op jit(solution)/shard_map/ppermute | solution.py:370
  47.7 68.3 %copy-start.35 = (bf16[512,256]{1,0:T(8,128)(2,1)}, bf16[512,256]{1,0:T(8,128)(2,1)S(1)}, u32[]{:S(2)}) copy-start(bf16[512,256]{1,0:T(8,128)(2,1)S(1)} %collective-permute-done.8.rest_1_) | copy-start | bytes 786436
  47.7 10.2 %collective-permute-start.9 = (bf16[512,256]{1,0:T(8,128)(2,1)S(1)}, bf16[512,256]{1,0:T(8,128)(2,1)}, u32[]{:S(2)}, u32[]{:S(2)}) collective-permute-start(bf16[512,256]{1,0:T(8,128)(2,1)S(1)} %collective-permute-done.8.rest_1_), channel_id=1, source_target_pairs={{0,4},{2,6},{4,12},{6,14},{12,8},{14,10},{8,0},{10,2},{1,5},{3,7},... | collective-permute-start | bytes 786440 | tf_op jit(solution)/shard_map/ppermute | solution.py:370
  48.5 13.3 %collective-permute-start.4 = (bf16[256,1024]{1,0:T(8,128)(2,1)S(1)}, bf16[256,1024]{1,0:T(8,128)(2,1)}, u32[]{:S(2)}, u32[]{:S(2)}) collective-permute-start(bf16[256,1024]{1,0:T(8,128)(2,1)S(1)} %pad_maximum_fusion.1.rest_2_), channel_id=1, source_target_pairs={{0,2},{2,0},{4,6},{6,4},{8,10},{10,8},{12,14},{14,12},{1,3},{3,1},... | collective-permute-start | bytes 1572872 | tf_op jit(solution)/shard_map/ppermute | solution.py:377
  50.0 24.9 %collective-permute-start.3 = (bf16[256,1024]{1,0:T(8,128)(2,1)}, bf16[256,1024]{1,0:T(8,128)(2,1)}, u32[]{:S(2)}, u32[]{:S(2)}) collective-permute-start(bf16[256,1024]{1,0:T(8,128)(2,1)} %collective-permute-done.2.rest_4_), channel_id=1, source_target_pairs={{0,4},{2,6},{4,12},{6,14},{12,8},{14,10},{8,0},{10,2},{1,5},{3,7},... | collective-permute-start | bytes 1572872 | tf_op jit(solution)/shard_map/ppermute | solution.py:370
  53.4 79.0 %collective-permute-start = (bf16[768,1024]{1,0:T(8,128)(2,1)S(1)}, bf16[768,1024]{1,0:T(8,128)(2,1)}, u32[]{:S(2)}, u32[]{:S(2)}) collective-permute-start(bf16[768,1024]{1,0:T(8,128)(2,1)S(1)} %bitcast.7), channel_id=1, source_target_pairs={{0,1},{1,0},{2,3},{3,2},{4,5},{5,4},{6,7},{7,6},{8,9},{9,8},{10,11... | collective-permute-start | bytes 4718600 | tf_op jit(solution)/shard_map/ppermute | solution.py:365
  57.8 15.7 %collective-permute-start.10 = (bf16[512,256]{1,0:T(8,128)(2,1)}, bf16[512,256]{1,0:T(8,128)(2,1)}, u32[]{:S(2)}, u32[]{:S(2)}) collective-permute-start(bf16[512,256]{1,0:T(8,128)(2,1)} %collective-permute-done.9.rest_2_), channel_id=1, source_target_pairs={{0,4},{2,6},{4,12},{6,14},{12,8},{14,10},{8,0},{10,2},{1,5},{3,7},... | collective-permute-start | bytes 786440 | tf_op jit(solution)/shard_map/ppermute | solution.py:370
  61.8 18.2 %collective-permute-start.5 = (bf16[256,1024]{1,0:T(8,128)(2,1)}, bf16[256,1024]{1,0:T(8,128)(2,1)}, u32[]{:S(2)}, u32[]{:S(2)}) collective-permute-start(bf16[256,1024]{1,0:T(8,128)(2,1)} %collective-permute-done.1.rest_3_), channel_id=1, source_target_pairs={{0,2},{2,0},{4,6},{6,4},{8,10},{10,8},{12,14},{14,12},{1,3},{3,1},... | collective-permute-start | bytes 1572872 | tf_op jit(solution)/shard_map/ppermute | solution.py:377
  73.6 15.1 %collective-permute-start.6 = (bf16[256,1024]{1,0:T(8,128)(2,1)}, bf16[256,1024]{1,0:T(8,128)(2,1)}, u32[]{:S(2)}, u32[]{:S(2)}) collective-permute-start(bf16[256,1024]{1,0:T(8,128)(2,1)} %collective-permute-done.2.rest_4_), channel_id=1, source_target_pairs={{0,2},{2,0},{4,6},{6,4},{8,10},{10,8},{12,14},{14,12},{1,3},{3,1},... | collective-permute-start | bytes 1572872 | tf_op jit(solution)/shard_map/ppermute | solution.py:377
  75.0 25.0 %collective-permute-start.7 = (bf16[256,1024]{1,0:T(8,128)(2,1)}, bf16[256,1024]{1,0:T(8,128)(2,1)}, u32[]{:S(2)}, u32[]{:S(2)}) collective-permute-start(bf16[256,1024]{1,0:T(8,128)(2,1)} %collective-permute-done.3.rest_5_), channel_id=1, source_target_pairs={{0,2},{2,0},{4,6},{6,4},{8,10},{10,8},{12,14},{14,12},{1,3},{3,1},... | collective-permute-start | bytes 1572872 | tf_op jit(solution)/shard_map/ppermute | solution.py:377
  77.6 38.4 %copy-start.14 = (bf16[4,128,256]{2,1,0:T(8,128)(2,1)}, bf16[4,128,256]{2,1,0:T(8,128)(2,1)S(1)}, u32[]{:S(2)}) copy-start(bf16[4,128,256]{2,1,0:T(8,128)(2,1)S(1)} %pad_maximum_fusion.2.gates_ref) | copy-start | bytes 786436
  80.0 35.9 %collective-permute-start.11 = (bf16[512,256]{1,0:T(8,128)(2,1)S(1)}, bf16[512,256]{1,0:T(8,128)(2,1)S(1)}, u32[]{:S(2)}, u32[]{:S(2)}) collective-permute-start(bf16[512,256]{1,0:T(8,128)(2,1)S(1)} %constant_dynamic-slice_fusion.9.rest_0_), channel_id=1, source_target_pairs={{0,2},{2,0},{4,6},{6,4},{8,10},{10,8},{12,14},{14,12},{1,3},{3,1},... | collective-permute-start | bytes 786440 | tf_op jit(solution)/shard_map/ppermute | solution.py:377
  88.7 27.3 %collective-permute-start.12 = (bf16[512,256]{1,0:T(8,128)(2,1)S(1)}, bf16[512,256]{1,0:T(8,128)(2,1)S(1)}, u32[]{:S(2)}, u32[]{:S(2)}) collective-permute-start(bf16[512,256]{1,0:T(8,128)(2,1)S(1)} %collective-permute-done.8.rest_1_), channel_id=1, source_target_pairs={{0,2},{2,0},{4,6},{6,4},{8,10},{10,8},{12,14},{14,12},{1,3},{3,1},... | collective-permute-start | bytes 786440 | tf_op jit(solution)/shard_map/ppermute | solution.py:377
  99.9 16.7 %collective-permute-start.13 = (bf16[512,256]{1,0:T(8,128)(2,1)}, bf16[512,256]{1,0:T(8,128)(2,1)S(1)}, u32[]{:S(2)}, u32[]{:S(2)}) collective-permute-start(bf16[512,256]{1,0:T(8,128)(2,1)} %collective-permute-done.9.rest_2_), channel_id=1, source_target_pairs={{0,2},{2,0},{4,6},{6,4},{8,10},{10,8},{12,14},{14,12},{1,3},{3,1},... | collective-permute-start | bytes 786440 | tf_op jit(solution)/shard_map/ppermute | solution.py:377
  101.3 19.0 %collective-permute-start.14 = (bf16[512,256]{1,0:T(8,128)(2,1)}, bf16[512,256]{1,0:T(8,128)(2,1)S(1)}, u32[]{:S(2)}, u32[]{:S(2)}) collective-permute-start(bf16[512,256]{1,0:T(8,128)(2,1)} %collective-permute-done.10.rest_3_), channel_id=1, source_target_pairs={{0,2},{2,0},{4,6},{6,4},{8,10},{10,8},{12,14},{14,12},{1,3},{3,1},... | collective-permute-start | bytes 786440 | tf_op jit(solution)/shard_map/ppermute | solution.py:377
  127.1 26.7 %collective-permute-start.21 = (bf16[384,1024]{1,0:T(8,128)(2,1)}, bf16[384,1024]{1,0:T(8,128)(2,1)}, u32[]{:S(2)}, u32[]{:S(2)}) collective-permute-start(bf16[384,1024]{1,0:T(8,128)(2,1)} %get-tuple-element.29), channel_id=1, source_target_pairs={{0,1},{1,0},{2,3},{3,2},{4,5},{5,4},{6,7},{7,6},{8,9},{9,8},{10,11... | collective-permute-start | bytes 2359304 | tf_op jit(solution)/shard_map/ppermute | solution.py:365
  130.1 34.6 %collective-permute-start.25 = (bf16[256,1408]{1,0:T(8,128)(2,1)}, bf16[256,1408]{1,0:T(8,128)(2,1)S(1)}, u32[]{:S(2)}, u32[]{:S(2)}) collective-permute-start(bf16[256,1408]{1,0:T(8,128)(2,1)} %concatenate.18.rest_4_.rest_2_.rest_3_), channel_id=1, source_target_pairs={{0,4},{2,6},{4,12},{6,14},{12,8},{14,10},{8,0},{10,2},{1,5},{3,7},... | collective-permute-start | bytes 2162696 | tf_op jit(solution)/shard_map/ppermute | solution.py:370
  134.4 13.7 %copy-start.45 = (bf16[512,256]{1,0:T(8,128)(2,1)S(1)}, bf16[512,256]{1,0:T(8,128)(2,1)}, u32[]{:S(2)}) copy-start(bf16[512,256]{1,0:T(8,128)(2,1)} %copy-done.44) | copy-start | bytes 786436
  151.6 14.6 %collective-permute-start.20 = (bf16[384,1024]{1,0:T(8,128)(2,1)S(1)}, bf16[384,1024]{1,0:T(8,128)(2,1)S(1)}, u32[]{:S(2)}, u32[]{:S(2)}) collective-permute-start(bf16[384,1024]{1,0:T(8,128)(2,1)S(1)} %get-tuple-element.27), channel_id=1, source_target_pairs={{0,1},{1,0},{2,3},{3,2},{4,5},{5,4},{6,7},{7,6},{8,9},{9,8},{10,11... | collective-permute-start | bytes 2359304 | tf_op jit(solution)/shard_map/ppermute | solution.py:365
  151.9 12.5 %collective-permute-start.18 = (bf16[384,1024]{1,0:T(8,128)(2,1)S(1)}, bf16[384,1024]{1,0:T(8,128)(2,1)S(1)}, u32[]{:S(2)}, u32[]{:S(2)}) collective-permute-start(bf16[384,1024]{1,0:T(8,128)(2,1)S(1)} %copy-done.17), channel_id=1, source_target_pairs={{0,1},{1,0},{2,3},{3,2},{4,5},{5,4},{6,7},{7,6},{8,9},{9,8},{10,11... | collective-permute-start | bytes 2359304 | tf_op jit(solution)/shard_map/ppermute | solution.py:365
  152.2 10.6 %collective-permute-start.32 = (bf16[704,256]{1,0:T(8,128)(2,1)S(1)}, bf16[704,256]{1,0:T(8,128)(2,1)S(1)}, u32[]{:S(2)}, u32[]{:S(2)}) collective-permute-start(bf16[704,256]{1,0:T(8,128)(2,1)S(1)} %constant_dynamic-slice_fusion.4), channel_id=1, source_target_pairs={{0,2},{2,0},{4,6},{6,4},{8,10},{10,8},{12,14},{14,12},{1,3},{3,1},... | collective-permute-start | bytes 1081352 | tf_op jit(solution)/shard_map/ppermute | solution.py:380
  155.2 20.5 %copy-start.6 = (bf16[256,1408]{1,0:T(8,128)(2,1)S(1)}, bf16[256,1408]{1,0:T(8,128)(2,1)}, u32[]{:S(2)}) copy-start(bf16[256,1408]{1,0:T(8,128)(2,1)} %concatenate.18.rest_4_.rest_2_.rest_3_) | copy-start | bytes 2162692
  155.2 20.5 %collective-permute-start.22 = (bf16[384,1024]{1,0:T(8,128)(2,1)S(1)}, bf16[384,1024]{1,0:T(8,128)(2,1)S(1)}, u32[]{:S(2)}, u32[]{:S(2)}) collective-permute-start(bf16[384,1024]{1,0:T(8,128)(2,1)S(1)} %shard_map.169), channel_id=1, source_target_pairs={{0,16},{16,0},{1,17},{17,1},{2,18},{18,2},{3,19},{19,3},{4,20},{20... | collective-permute-start | bytes 2359304 | tf_op jit(solution)/shard_map/ppermute | solution.py:362
  162.9 13.8 %copy-start.9 = (bf16[1408,256]{1,0:T(8,128)(2,1)}, bf16[1408,256]{1,0:T(8,128)(2,1)S(1)}, u32[]{:S(2)}) copy-start(bf16[1408,256]{1,0:T(8,128)(2,1)S(1)} %pad_maximum_fusion.rest_12_.rest_10_.rest_11_) | copy-start | bytes 2162692
  162.9 20.0 %collective-permute-start.33 = (bf16[1408,256]{1,0:T(8,128)(2,1)S(1)}, bf16[1408,256]{1,0:T(8,128)(2,1)S(1)}, u32[]{:S(2)}, u32[]{:S(2)}) collective-permute-start(bf16[1408,256]{1,0:T(8,128)(2,1)S(1)} %pad_maximum_fusion.rest_12_.rest_10_.rest_11_), channel_id=1, source_target_pairs={{0,4},{2,6},{4,12},{6,14},{12,8},{14,10},{8,0},{10,2},{1,5},{3,7},... | collective-permute-start | bytes 2162696 | tf_op jit(solution)/shard_map/ppermute | solution.py:370
  164.4 33.9 %collective-permute-start.15 = (bf16[384,1024]{1,0:T(8,128)(2,1)S(1)}, bf16[384,1024]{1,0:T(8,128)(2,1)S(1)}, u32[]{:S(2)}, u32[]{:S(2)}) collective-permute-start(bf16[384,1024]{1,0:T(8,128)(2,1)S(1)} %get-tuple-element.23), channel_id=1, source_target_pairs={{0,1},{1,0},{2,3},{3,2},{4,5},{5,4},{6,7},{7,6},{8,9},{9,8},{10,11... | collective-permute-start | bytes 2359304 | tf_op jit(solution)/shard_map/ppermute | solution.py:365
  164.7 32.1 %copy-start.20 = (bf16[256,1408]{1,0:T(8,128)(2,1)}, bf16[256,1408]{1,0:T(8,128)(2,1)S(1)}, u32[]{:S(2)}) copy-start(bf16[256,1408]{1,0:T(8,128)(2,1)S(1)} %collective-permute-done.25.rest_5_.rest_3_.rest_4_) | copy-start | bytes 2162692
  164.7 34.2 %collective-permute-start.19 = (bf16[384,1024]{1,0:T(8,128)(2,1)S(1)}, bf16[384,1024]{1,0:T(8,128)(2,1)S(1)}, u32[]{:S(2)}, u32[]{:S(2)}) collective-permute-start(bf16[384,1024]{1,0:T(8,128)(2,1)S(1)} %shard_map.167), channel_id=1, source_target_pairs={{0,16},{16,0},{1,17},{17,1},{2,18},{18,2},{3,19},{19,3},{4,20},{20... | collective-permute-start | bytes 2359304 | tf_op jit(solution)/shard_map/ppermute | solution.py:362
  166.2 30.6 %collective-permute-start.26 = (bf16[256,1408]{1,0:T(8,128)(2,1)S(1)}, bf16[256,1408]{1,0:T(8,128)(2,1)}, u32[]{:S(2)}, u32[]{:S(2)}) collective-permute-start(bf16[256,1408]{1,0:T(8,128)(2,1)S(1)} %collective-permute-done.25.rest_5_.rest_3_.rest_4_), channel_id=1, source_target_pairs={{0,4},{2,6},{4,12},{6,14},{12,8},{14,10},{8,0},{10,2},{1,5},{3,7},... | collective-permute-start | bytes 2162696 | tf_op jit(solution)/shard_map/ppermute | solution.py:370
  175.7 25.1 %collective-permute-start.28 = (bf16[256,1408]{1,0:T(8,128)(2,1)S(1)}, bf16[256,1408]{1,0:T(8,128)(2,1)S(1)}, u32[]{:S(2)}, u32[]{:S(2)}) collective-permute-start(bf16[256,1408]{1,0:T(8,128)(2,1)S(1)} %copy-done.6), channel_id=1, source_target_pairs={{0,2},{2,0},{4,6},{6,4},{8,10},{10,8},{12,14},{14,12},{1,3},{3,1},... | collective-permute-start | bytes 2162696 | tf_op jit(solution)/shard_map/ppermute | solution.py:377
  182.8 17.9 %copy-start.23 = (bf16[1408,256]{1,0:T(8,128)(2,1)}, bf16[1408,256]{1,0:T(8,128)(2,1)S(1)}, u32[]{:S(2)}) copy-start(bf16[1408,256]{1,0:T(8,128)(2,1)S(1)} %collective-permute-done.33.rest_13_.rest_11_.rest_12_) | copy-start | bytes 2162692
  182.9 26.6 %collective-permute-start.37 = (bf16[384,1024]{1,0:T(8,128)(2,1)S(1)}, bf16[384,1024]{1,0:T(8,128)(2,1)}, u32[]{:S(2)}, u32[]{:S(2)}) collective-permute-start(bf16[384,1024]{1,0:T(8,128)(2,1)S(1)} %shard_map.170.rest_0_.refs_0_), channel_id=1, source_target_pairs={{0,16},{16,0},{1,17},{17,1},{2,18},{18,2},{3,19},{19,3},{4,20},{20... | collective-permute-start | bytes 2359304 | tf_op jit(solution)/shard_map/ppermute | solution.py:362
  196.8 16.6 %collective-permute-start.29 = (bf16[256,1408]{1,0:T(8,128)(2,1)S(1)}, bf16[256,1408]{1,0:T(8,128)(2,1)S(1)}, u32[]{:S(2)}, u32[]{:S(2)}) collective-permute-start(bf16[256,1408]{1,0:T(8,128)(2,1)S(1)} %collective-permute-done.25.rest_5_.rest_3_.rest_4_), channel_id=1, source_target_pairs={{0,2},{2,0},{4,6},{6,4},{8,10},{10,8},{12,14},{14,12},{1,3},{3,1},... | collective-permute-start | bytes 2162696 | tf_op jit(solution)/shard_map/ppermute | solution.py:377
  198.3 20.0 %collective-permute-start.34 = (bf16[1408,256]{1,0:T(8,128)(2,1)S(1)}, bf16[1408,256]{1,0:T(8,128)(2,1)}, u32[]{:S(2)}, u32[]{:S(2)}) collective-permute-start(bf16[1408,256]{1,0:T(8,128)(2,1)S(1)} %collective-permute-done.33.rest_13_.rest_11_.rest_12_), channel_id=1, source_target_pairs={{0,4},{2,6},{4,12},{6,14},{12,8},{14,10},{8,0},{10,2},{1,5},{3,7},... | collective-permute-start | bytes 2162696 | tf_op jit(solution)/shard_map/ppermute | solution.py:370
  198.9 34.9 %collective-permute-start.27 = (bf16[256,1408]{1,0:T(8,128)(2,1)}, bf16[256,1408]{1,0:T(8,128)(2,1)}, u32[]{:S(2)}, u32[]{:S(2)}) collective-permute-start(bf16[256,1408]{1,0:T(8,128)(2,1)} %collective-permute-done.26.rest_6_.rest_4_.rest_5_), channel_id=1, source_target_pairs={{0,4},{2,6},{4,12},{6,14},{12,8},{14,10},{8,0},{10,2},{1,5},{3,7},... | collective-permute-start | bytes 2162696 | tf_op jit(solution)/shard_map/ppermute | solution.py:370
  200.3 34.0 %copy-start.48 = (f32[2048]{0:T(1024)S(1)}, f32[2048]{0:T(1024)}, u32[]{:S(2)}) copy-start(f32[2048]{0:T(1024)} %param.27) | copy-start | bytes 24580
  200.3 34.3 %copy-start.49 = (f32[3,1408]{1,0:T(4,128)S(1)}, f32[3,1408]{1,0:T(4,128)}, u32[]{:S(2)}) copy-start(f32[3,1408]{1,0:T(4,128)} %param.31) | copy-start | bytes 50692
  200.3 34.3 %copy-start.50 = (f32[3,1408]{1,0:T(4,128)S(1)}, f32[3,1408]{1,0:T(4,128)}, u32[]{:S(2)}) copy-start(f32[3,1408]{1,0:T(4,128)} %param.30) | copy-start | bytes 50692
  201.8 32.5 %collective-permute-start.39 = (bf16[384,1024]{1,0:T(8,128)(2,1)S(1)}, bf16[384,1024]{1,0:T(8,128)(2,1)}, u32[]{:S(2)}, u32[]{:S(2)}) collective-permute-start(bf16[384,1024]{1,0:T(8,128)(2,1)S(1)} %shard_map.168.rest_1_.refs_0_), channel_id=1, source_target_pairs={{0,16},{16,0},{1,17},{17,1},{2,18},{18,2},{3,19},{19,3},{4,20},{20... | collective-permute-start | bytes 2359304 | tf_op jit(solution)/shard_map/ppermute | solution.py:362
  209.5 37.3 %collective-permute-start.38 = (bf16[384,1024]{1,0:T(8,128)(2,1)}, bf16[384,1024]{1,0:T(8,128)(2,1)S(1)}, u32[]{:S(2)}, u32[]{:S(2)}) collective-permute-start(bf16[384,1024]{1,0:T(8,128)(2,1)} %collective-permute-done.37.rest_0_), channel_id=1, source_target_pairs={{0,1},{1,0},{2,3},{3,2},{4,5},{5,4},{6,7},{7,6},{8,9},{9,8},{10,11... | collective-permute-start | bytes 2359304 | tf_op jit(solution)/shard_map/ppermute | solution.py:365
  214.3 20.5 %collective-permute-start.30 = (bf16[256,1408]{1,0:T(8,128)(2,1)}, bf16[256,1408]{1,0:T(8,128)(2,1)S(1)}, u32[]{:S(2)}, u32[]{:S(2)}) collective-permute-start(bf16[256,1408]{1,0:T(8,128)(2,1)} %collective-permute-done.26.rest_6_.rest_4_.rest_5_), channel_id=1, source_target_pairs={{0,2},{2,0},{4,6},{6,4},{8,10},{10,8},{12,14},{14,12},{1,3},{3,1},... | collective-permute-start | bytes 2162696 | tf_op jit(solution)/shard_map/ppermute | solution.py:377
  218.4 28.2 %collective-permute-start.35 = (bf16[1408,256]{1,0:T(8,128)(2,1)}, bf16[1408,256]{1,0:T(8,128)(2,1)}, u32[]{:S(2)}, u32[]{:S(2)}) collective-permute-start(bf16[1408,256]{1,0:T(8,128)(2,1)} %collective-permute-done.34.rest_14_.rest_12_.rest_13_), channel_id=1, source_target_pairs={{0,4},{2,6},{4,12},{6,14},{12,8},{14,10},{8,0},{10,2},{1,5},{3,7},... | collective-permute-start | bytes 2162696 | tf_op jit(solution)/shard_map/ppermute | solution.py:370
  233.8 13.0 %collective-permute-start.31 = (bf16[256,1408]{1,0:T(8,128)(2,1)}, bf16[256,1408]{1,0:T(8,128)(2,1)}, u32[]{:S(2)}, u32[]{:S(2)}) collective-permute-start(bf16[256,1408]{1,0:T(8,128)(2,1)} %collective-permute-done.27.rest_7_.rest_5_.rest_6_), channel_id=1, source_target_pairs={{0,2},{2,0},{4,6},{6,4},{8,10},{10,8},{12,14},{14,12},{1,3},{3,1},... | collective-permute-start | bytes 2162696 | tf_op jit(solution)/shard_map/ppermute | solution.py:377
  234.3 31.8 %collective-permute-start.40 = (bf16[384,1024]{1,0:T(8,128)(2,1)}, bf16[384,1024]{1,0:T(8,128)(2,1)}, u32[]{:S(2)}, u32[]{:S(2)}) collective-permute-start(bf16[384,1024]{1,0:T(8,128)(2,1)} %collective-permute-done.39.rest_1_), channel_id=1, source_target_pairs={{0,1},{1,0},{2,3},{3,2},{4,5},{5,4},{6,7},{7,6},{8,9},{9,8},{10,11... | collective-permute-start | bytes 2359304 | tf_op jit(solution)/shard_map/ppermute | solution.py:365
  235.6 39.8 %collective-permute-start.23 = (bf16[384,1024]{1,0:T(8,128)(2,1)S(1)}, bf16[384,1024]{1,0:T(8,128)(2,1)}, u32[]{:S(2)}, u32[]{:S(2)}) collective-permute-start(bf16[384,1024]{1,0:T(8,128)(2,1)S(1)} %shard_map.170.rest_0_.refs_0_), channel_id=1, source_target_pairs={{0,1},{1,0},{2,3},{3,2},{4,5},{5,4},{6,7},{7,6},{8,9},{9,8},{10,11... | collective-permute-start | bytes 2359304 | tf_op jit(solution)/shard_map/ppermute | solution.py:365
  246.5 28.9 %collective-permute-start.24 = (bf16[384,1024]{1,0:T(8,128)(2,1)}, bf16[384,1024]{1,0:T(8,128)(2,1)}, u32[]{:S(2)}, u32[]{:S(2)}) collective-permute-start(bf16[384,1024]{1,0:T(8,128)(2,1)} %copy-done.2), channel_id=1, source_target_pairs={{0,1},{1,0},{2,3},{3,2},{4,5},{5,4},{6,7},{7,6},{8,9},{9,8},{10,11... | collective-permute-start | bytes 2359304 | tf_op jit(solution)/shard_map/ppermute | solution.py:365
  265.7 25.1 %collective-permute-start.44 = (bf16[384,1024]{1,0:T(8,128)(2,1)S(1)}, bf16[384,1024]{1,0:T(8,128)(2,1)S(1)}, u32[]{:S(2)}, u32[]{:S(2)}) collective-permute-start(bf16[384,1024]{1,0:T(8,128)(2,1)S(1)} %get-tuple-element.38), channel_id=1, source_target_pairs={{0,1},{1,0},{2,3},{3,2},{4,5},{5,4},{6,7},{7,6},{8,9},{9,8},{10,11... | collective-permute-start | bytes 2359304 | tf_op jit(solution)/shard_map/ppermute | solution.py:365
  275.2 17.5 %collective-permute-start.41 = (bf16[384,1024]{1,0:T(8,128)(2,1)S(1)}, bf16[384,1024]{1,0:T(8,128)(2,1)S(1)}, u32[]{:S(2)}, u32[]{:S(2)}) collective-permute-start(bf16[384,1024]{1,0:T(8,128)(2,1)S(1)} %get-tuple-element.34), channel_id=1, source_target_pairs={{0,1},{1,0},{2,3},{3,2},{4,5},{5,4},{6,7},{7,6},{8,9},{9,8},{10,11... | collective-permute-start | bytes 2359304 | tf_op jit(solution)/shard_map/ppermute | solution.py:365
  290.4 3.1 collective-permute-start.43
  291.1 20.5 %collective-permute-start.45 = (bf16[384,1024]{1,0:T(8,128)(2,1)S(1)}, bf16[384,1024]{1,0:T(8,128)(2,1)S(1)}, u32[]{:S(2)}, u32[]{:S(2)}) collective-permute-start(bf16[384,1024]{1,0:T(8,128)(2,1)S(1)} %shard_map.175), channel_id=1, source_target_pairs={{0,16},{16,0},{1,17},{17,1},{2,18},{18,2},{3,19},{19,3},{4,20},{20... | collective-permute-start | bytes 2359304 | tf_op jit(solution)/shard_map/ppermute | solution.py:362
  292.6 20.3 %collective-permute-start.36 = (bf16[384,1024]{1,0:T(8,128)(2,1)S(1)}, bf16[384,1024]{1,0:T(8,128)(2,1)S(1)}, u32[]{:S(2)}, u32[]{:S(2)}) collective-permute-start(bf16[384,1024]{1,0:T(8,128)(2,1)S(1)} %get-tuple-element.31), channel_id=1, source_target_pairs={{0,1},{1,0},{2,3},{3,2},{4,5},{5,4},{6,7},{7,6},{8,9},{9,8},{10,11... | collective-permute-start | bytes 2359304 | tf_op jit(solution)/shard_map/ppermute | solution.py:365
  292.9 34.7 %collective-permute-start.42 = (bf16[384,1024]{1,0:T(8,128)(2,1)S(1)}, bf16[384,1024]{1,0:T(8,128)(2,1)S(1)}, u32[]{:S(2)}, u32[]{:S(2)}) collective-permute-start(bf16[384,1024]{1,0:T(8,128)(2,1)S(1)} %shard_map.174), channel_id=1, source_target_pairs={{0,16},{16,0},{1,17},{17,1},{2,18},{18,2},{3,19},{19,3},{4,20},{20... | collective-permute-start | bytes 2359304 | tf_op jit(solution)/shard_map/ppermute | solution.py:362
  (36 other events, 196.8 us)

commit v2 on v1

--- a/solution.py
+++ b/solution.py
@@ -176,16 +176,15 @@
         for start, ref in zip(starts, refs):
             term = ref[pl.ds(pl.multiple_of(start + at, TILE), TILE), :].astype(F32)
             total = term if total is None else total + term
-        out_ref[pl.ds(at, TILE), :] = total.astype(BF16)
+        out_ref[pl.ds(at, TILE), :] = total.astype(out_ref.dtype)
         return 0
 
-    lax.fori_loop(0, out_ref.shape[0] // TILE, step, 0, unroll=2)
+    lax.fori_loop(0, out_ref.shape[0] // TILE, step, 0, unroll=4)
 
 
 def final_kernel(start, chained, *refs):
-    terms = refs[:4]
-    out_ref, buffer_ref, sem = refs[4 + chained :]
-    add_kernel([0] * 4, *terms, buffer_ref)
+    out_ref, buffer_ref, sem = refs[2 + chained :]
+    add_kernel([0] * 2, *refs[:2], buffer_ref)
     copy = pltpu.make_async_copy(buffer_ref, out_ref.at[pl.ds(start, buffer_ref.shape[0])], sem)
     copy.start()
     copy.wait()
@@ -206,7 +205,7 @@
     stream_copies = fetch_streams(streams, buffers, sems, n_pieces)
     copies = fetch_rows(order_ref, pieces, wbuf, sems)
     down_copies = fetch_blocks(order_ref, downs, down_ref, sems, n_pieces + n_streams)
-    for copy in stream_copies + copies + down_copies:
+    for copy in stream_copies + copies:
         copy.start()
     clear_padding(downs, down_ref)
     for copy in stream_copies:
@@ -218,6 +217,8 @@
     norm_into(own_ref, peer_ref, gain_ref, normed_ref)
     for copy in copies:
         copy.wait()
+    for copy in down_copies:
+        copy.start()
     rows = row_block(length)
     pre_ref[0:8, :] = before_ref[...] if halo else jnp.zeros((8, width), F32)
     low = lax.broadcasted_iota(jnp.int32, (TILE, 128), 1) < 64
@@ -407,7 +408,10 @@
     out_pieces = gather_z_first(half_of(out_weight, 0))
     both = interleave(gate_weight, up_weight)
     ffn_pieces = gather_z_first(both)
-    down_pieces = gather_y_first(half_of(down_weight, 0))
+    down_pieces = [
+        pltpu.with_memory_space_constraint(piece, pltpu.HBM)
+        for piece in gather_y_first(half_of(down_weight, 0))
+    ]
 
     gates = jnp.concatenate([half_of(rate_blocks, 0), half_of(admit_blocks, 0)], axis=2)
     slope = -GATE_SCALE * jax.nn.softplus(-half_of(decay_logit, 0))[None]
@@ -432,7 +436,7 @@
                 pltpu.VMEM((length, channels), F32),
                 pltpu.VMEM((length, 2 * channels), F32),
             ],
-            30,
+            22,
             length * 2 * half * 2 * channels * 2,
             [order, gain, taps, gates, slope, out_gain],
             [stream, peer] + mix_pieces,
@@ -446,7 +450,7 @@
             functools.partial(out_kernel, parts),
             sums,
             [pltpu.VMEM((n_fs, depth, pieces[0].shape[1]), BF16)],
-            16,
+            10,
             rows * depth * 2 * half * 2,
             [order, left],
             pieces,
@@ -473,7 +477,7 @@
                 pltpu.VMEM((rows, padded_units), BF16),
                 pltpu.VMEM((n_fs, padded_units, down_pieces[0].shape[1]), BF16),
             ],
-            36,
+            20 if parts == 1 else 28,
             rows * 2 * half * width * 3,
             [order, gain2, ffn_taps] + halo,
             pieces,
@@ -481,12 +485,12 @@
         )
         return outs[:parts], outs[parts : 2 * parts], outs[2 * parts]
 
-    def add(*terms):
+    def add(*terms, dtype=BF16):
         starts = [t[1] if isinstance(t, tuple) else 0 for t in terms]
         arrays = [t[0] if isinstance(t, tuple) else t for t in terms]
         return pl.pallas_call(
             functools.partial(add_kernel, starts),
-            out_shape=jax.ShapeDtypeStruct((part, half), BF16),
+            out_shape=jax.ShapeDtypeStruct((part, half), dtype),
             in_specs=[VMEM] * len(arrays),
             out_specs=VMEM,
             compiler_params=pltpu.CompilerParams(vmem_limit_bytes=12 * 1024 * 1024),
@@ -516,18 +520,18 @@
     keeps, sends, _ = ffn(middle, middle_peer, None)
     result = []
     for i in range(PARTS):
-        terms = [middle[i], keeps[i], partner(sends[i]), sent[i]]
+        local_sum = add(middle[i], keeps[i], partner(sends[i]), dtype=F32)
         run = pl.pallas_call(
             functools.partial(final_kernel, i * part, len(result)),
             out_shape=jax.ShapeDtypeStruct((length, half), BF16),
-            in_specs=[VMEM] * 4 + [HBM] * len(result),
+            in_specs=[VMEM] * 2 + [HBM] * len(result),
             out_specs=HBM,
             scratch_shapes=[pltpu.VMEM((part, half), BF16), pltpu.SemaphoreType.DMA],
-            input_output_aliases={4: 0} if result else {},
+            input_output_aliases={2: 0} if result else {},
             compiler_params=pltpu.CompilerParams(vmem_limit_bytes=12 * 1024 * 1024),
             cost_estimate=pl.CostEstimate(flops=part * half * 4, bytes_accessed=2**21, transcendentals=0),
         )
-        result = [run(*terms, *result)]
+        result = [run(local_sum, sent[i], *result)]
     return result[0][None]
 
 

time: 330 us -> 327 us (level)
    unnamed x108 -> x100, local copies, waits for them, and re-layouts: 17.4 us -> 15.1 us
where the time goes in v2:
time: 327 us; the launch traced here: 326 us
  waiting for transfers between devices  182 us (56%)
  Pallas kernels  72.7 us (22%)
  starting transfers between devices  44.4 us (14%)
  local copies, waits for them, and re-layouts  24.8 us (8%)
    ppermute x12, waiting for transfers between devices, around(): found[k] = lax.ppermute(found[k - 1], 'fs', ring_pairs)  82.6 us
    pallas_call x7, Pallas kernels, call(): pl.pallas_call(functools.partial(kernel, len(pieces)), out_shape=outs, in...  67 us
    ppermute x7, waiting for transfers between devices, across(): return lax.ppermute(value, 'rep', flip)  66.3 us
    ppermute x12, waiting for transfers between devices, gather_z_first(): return found + [lax.ppermute(q, 'fs', swap_pairs) for q in found]  27 us
    ppermute x12, starting transfers between devices, around(): found[k] = lax.ppermute(found[k - 1], 'fs', ring_pairs)  15.2 us
    unnamed x100, local copies, waits for them, and re-layouts  15.1 us
    ppermute x12, starting transfers between devices, gather_z_first(): return found + [lax.ppermute(q, 'fs', swap_pairs) for q in found]  14 us
    ppermute x7, starting transfers between devices, across(): return lax.ppermute(value, 'rep', flip)  11.3 us
  transfers between devices with their start and end apart: 46, of which 22 were waited for; matrix products, arithmetic and copies ran while one was open for 3% of the time, Pallas kernels for 22%

profile of v2, /device:TPU:0, one launch (start us, length us, event | category | flops | bytes accessed | tf_op | source)
XLA Modules:
  0.0 325.9 jit_solution(15204117214839807949)
XLA Ops:
  0.0 3.0 collective-permute-start.16
  3.1 1.1 constant_dynamic-slice_fusion.10
  4.3 1.6 collective-permute-start.1
  5.9 12.8 %collective-permute-done.1.rest_3_ = bf16[256,1024]{1,0:T(8,128)(2,1)} collective-permute-done((bf16[256,1024]{1,0:T(8,128)(2,1)S(1)}, bf16[256,1024]{1,0:T(8,128)(2,1)}, u32[]{:S(2)}, u32[]{:S(2)}) %collective-permute-start.1) | collective-permute-done | bytes 524320 | tf_op jit(solution)/shard_map/ppermute | solution.py:371
  19.4 18.4 %collective-permute-done.16.rest_0_ = bf16[768,1024]{1,0:T(8,128)(2,1)} collective-permute-done((bf16[768,1024]{1,0:T(8,128)(2,1)}, bf16[768,1024]{1,0:T(8,128)(2,1)}, u32[]{:S(2)}, u32[]{:S(2)}) %collective-permute-start.16) | collective-permute-done | bytes 1572896 | tf_op jit(solution)/shard_map/ppermute | solution.py:363
  37.8 1.9 collective-permute-start.8
  39.7 8.0 %collective-permute-done.8.rest_1_ = bf16[512,256]{1,0:T(8,128)(2,1)S(1)} collective-permute-done((bf16[512,256]{1,0:T(8,128)(2,1)S(1)}, bf16[512,256]{1,0:T(8,128)(2,1)S(1)}, u32[]{:S(2)}, u32[]{:S(2)}) %collective-permute-start.8) | collective-permute-done | bytes 262176 | tf_op jit(solution)/shard_map/ppermute | solution.py:371
  48.5 1.5 collective-permute-start.4
  50.0 3.4 %collective-permute-start.3 = (bf16[256,1024]{1,0:T(8,128)(2,1)}, bf16[256,1024]{1,0:T(8,128)(2,1)}, u32[]{:S(2)}, u32[]{:S(2)}) collective-permute-start(bf16[256,1024]{1,0:T(8,128)(2,1)} %collective-permute-done.2.rest_4_), channel_id=1, source_target_pairs={{0,4},{2,6},{4,12},{6,14},{12,8},{14,10},{8,0},{10,2},{1,5},{3,7},... | collective-permute-start | bytes 1572872 | tf_op jit(solution)/shard_map/ppermute | solution.py:371
  53.4 4.4 %collective-permute-done.9.rest_2_ = bf16[512,256]{1,0:T(8,128)(2,1)} collective-permute-done((bf16[512,256]{1,0:T(8,128)(2,1)S(1)}, bf16[512,256]{1,0:T(8,128)(2,1)}, u32[]{:S(2)}, u32[]{:S(2)}) %collective-permute-start.9) | collective-permute-done | bytes 262176 | tf_op jit(solution)/shard_map/ppermute | solution.py:371
  58.7 1.6 constant_dynamic-slice_fusion.12
  60.3 1.5 collective-permute-done.4.rest_6_
  61.8 1.5 collective-permute-start.5
  63.3 10.3 %collective-permute-done.10.rest_3_ = bf16[512,256]{1,0:T(8,128)(2,1)} collective-permute-done((bf16[512,256]{1,0:T(8,128)(2,1)}, bf16[512,256]{1,0:T(8,128)(2,1)}, u32[]{:S(2)}, u32[]{:S(2)}) %collective-permute-start.10) | collective-permute-done | bytes 262176 | tf_op jit(solution)/shard_map/ppermute | solution.py:371
  73.6 1.4 collective-permute-start.6
  77.6 2.4 constant_dynamic-slice_fusion
  80.0 1.4 collective-permute-start.11
  81.4 7.2 %collective-permute-done.6.rest_8_ = bf16[256,1024]{1,0:T(8,128)(2,1)} collective-permute-done((bf16[256,1024]{1,0:T(8,128)(2,1)}, bf16[256,1024]{1,0:T(8,128)(2,1)}, u32[]{:S(2)}, u32[]{:S(2)}) %collective-permute-start.6) | collective-permute-done | bytes 524320 | tf_op jit(solution)/shard_map/ppermute | solution.py:378
  88.7 1.4 collective-permute-start.12
  90.1 9.9 %collective-permute-done.7.rest_9_ = bf16[256,1024]{1,0:T(8,128)(2,1)} collective-permute-done((bf16[256,1024]{1,0:T(8,128)(2,1)}, bf16[256,1024]{1,0:T(8,128)(2,1)}, u32[]{:S(2)}, u32[]{:S(2)}) %collective-permute-start.7) | collective-permute-done | bytes 524320 | tf_op jit(solution)/shard_map/ppermute | solution.py:378
  99.9 1.4 collective-permute-start.13
  102.0 14.0 %shard_map.165.left_ref = bf16[768,512]{1,0:T(8,128)(2,1)S(1)} custom-call(s32[8]{0:T(128)S(1)} %fusion.1.order_ref, f32[2,1024]{1,0:T(2,128)S(1)} %broadcast_select_fusion.1.gain_ref, f32[4,512]{1,0:T(4,128)S(1)} %constant_dynamic-slice_fusion.14.taps_ref, bf16[4,128,256]{2,1,0:T(8,128)(2,1)S(1)} %pad_maximum_fusion.2.gates_ref, f32[1,512]{1,0:T(1,128)S(1)} %bitcast.11, ...), custom_call_target="tpu_custom_call" | custom-call | flops 3221225472 | bytes 4194304 | tf_op jit(solution)/shard_map/pallas_call | solution.py:304
  116.7 3.6 %collective-permute-done.14.rest_7_ = bf16[512,256]{1,0:T(8,128)(2,1)S(1)} collective-permute-done((bf16[512,256]{1,0:T(8,128)(2,1)}, bf16[512,256]{1,0:T(8,128)(2,1)S(1)}, u32[]{:S(2)}, u32[]{:S(2)}) %collective-permute-start.14) | collective-permute-done | bytes 262176 | tf_op jit(solution)/shard_map/ppermute | solution.py:378
  121.3 4.0 %shard_map.166 = (bf16[384,1024]{1,0:T(8,128)(2,1)S(1)}, bf16[384,1024]{1,0:T(8,128)(2,1)S(1)}, bf16[384,1024]{1,0:T(8,128)(2,1)}, bf16[384,1024]{1,0:T(8,128)(2,1)S(1)}) custom-call(s32[8]{0:T(128)S(1)} %fusion.1.order_ref, bf16[768,512]{1,0:T(8,128)(2,1)S(1)} %shard_map.165.left_ref, bf16[512,256]{1,0:T(8,128)(2,1)S(1)} %constant_dynamic-slice_fusion.9.rest_0_, ...), custom_call_target="tpu_custom_call" | custom-call | flops 1610612736 | bytes 4194304 | tf_op jit(solution)/shard_map/pallas_call | solution.py:304
  127.1 1.0 constant_dynamic-slice_fusion.5
  128.1 2.0 concatenate.18.rest_4_.rest_2_.rest_3_
  130.1 2.4 collective-permute-start.25
  132.4 1.0 copy-done.10
  134.5 13.6 %shard_map.163.left_ref = bf16[768,512]{1,0:T(8,128)(2,1)S(1)} custom-call(s32[8]{0:T(128)S(1)} %fusion.1.order_ref, f32[2,1024]{1,0:T(2,128)S(1)} %broadcast_select_fusion.1.gain_ref, f32[4,512]{1,0:T(4,128)S(1)} %constant_dynamic-slice_fusion.14.taps_ref, bf16[4,128,256]{2,1,0:T(8,128)(2,1)S(1)} %copy-done.12, f32[1,512]{1,0:T(1,128)S(1)} %bitcast.12, ...), custom_call_target="tpu_custom_call" | custom-call | flops 3221225472 | bytes 4194304 | tf_op jit(solution)/shard_map/pallas_call | solution.py:304
  148.1 3.5 %shard_map.164 = (bf16[384,1024]{1,0:T(8,128)(2,1)S(1)}, bf16[384,1024]{1,0:T(8,128)(2,1)S(1)}, bf16[384,1024]{1,0:T(8,128)(2,1)S(1)}, bf16[384,1024]{1,0:T(8,128)(2,1)S(1)}) custom-call(s32[8]{0:T(128)S(1)} %fusion.1.order_ref, bf16[768,512]{1,0:T(8,128)(2,1)S(1)} %shard_map.163.left_ref, bf16[512,256]{1,0:T(8,128)(2,1)S(1)} %constant_dynamic-slice_fusion.9.rest_0_, ...), custom_call_target="tpu_custom_call" | custom-call | flops 1610612736 | bytes 4194304 | tf_op jit(solution)/shard_map/pallas_call | solution.py:304
  152.2 1.6 collective-permute-start.32
  153.8 1.4 shard_map.169
  155.2 1.6 collective-permute-start.22
  156.8 6.1 %collective-permute-done.32 = bf16[704,256]{1,0:T(8,128)(2,1)S(1)} collective-permute-done((bf16[704,256]{1,0:T(8,128)(2,1)S(1)}, bf16[704,256]{1,0:T(8,128)(2,1)S(1)}, u32[]{:S(2)}, u32[]{:S(2)}) %collective-permute-start.32) | collective-permute-done | bytes 360480 | tf_op jit(solution)/shard_map/ppermute | solution.py:381
  162.9 1.5 collective-permute-start.33
  164.7 1.6 collective-permute-start.19
  166.5 9.2 %collective-permute-done.22.refs_3_ = bf16[384,1024]{1,0:T(8,128)(2,1)S(1)} collective-permute-done((bf16[384,1024]{1,0:T(8,128)(2,1)S(1)}, bf16[384,1024]{1,0:T(8,128)(2,1)S(1)}, u32[]{:S(2)}, u32[]{:S(2)}) %collective-permute-start.22) | collective-permute-done | bytes 786464 | tf_op jit(solution)/shard_map/ppermute | solution.py:363
  176.7 6.2 %collective-permute-done.33.rest_13_.rest_11_.rest_12_ = bf16[1408,256]{1,0:T(8,128)(2,1)S(1)} collective-permute-done((bf16[1408,256]{1,0:T(8,128)(2,1)S(1)}, bf16[1408,256]{1,0:T(8,128)(2,1)S(1)}, u32[]{:S(2)}, u32[]{:S(2)}) %collective-permute-start.33) | collective-permute-done | bytes 720928 | tf_op jit(solution)/shard_map/ppermute | solution.py:371
  182.9 1.5 collective-permute-start.37
  184.4 12.5 %collective-permute-done.26.rest_6_.rest_4_.rest_5_ = bf16[256,1408]{1,0:T(8,128)(2,1)} collective-permute-done((bf16[256,1408]{1,0:T(8,128)(2,1)S(1)}, bf16[256,1408]{1,0:T(8,128)(2,1)}, u32[]{:S(2)}, u32[]{:S(2)}) %collective-permute-start.26) | collective-permute-done | bytes 720928 | tf_op jit(solution)/shard_map/ppermute | solution.py:371
  196.8 1.5 collective-permute-start.29
  198.9 1.4 collective-permute-start.27
  200.8 1.0 copy-done.20
  201.7 1.5 collective-permute-start.39
  203.2 6.3 %collective-permute-done.37.rest_0_ = bf16[384,1024]{1,0:T(8,128)(2,1)} collective-permute-done((bf16[384,1024]{1,0:T(8,128)(2,1)S(1)}, bf16[384,1024]{1,0:T(8,128)(2,1)}, u32[]{:S(2)}, u32[]{:S(2)}) %collective-permute-start.37) | collective-permute-done | bytes 786464 | tf_op jit(solution)/shard_map/ppermute | solution.py:363
  209.5 3.9 %collective-permute-done.29.rest_9_.rest_7_.rest_8_ = bf16[256,1408]{1,0:T(8,128)(2,1)S(1)} collective-permute-done((bf16[256,1408]{1,0:T(8,128)(2,1)S(1)}, bf16[256,1408]{1,0:T(8,128)(2,1)S(1)}, u32[]{:S(2)}, u32[]{:S(2)}) %collective-permute-start.29) | collective-permute-done | bytes 720928 | tf_op jit(solution)/shard_map/ppermute | solution.py:378
  214.2 1.5 collective-permute-start.30
  215.8 2.6 collective-permute-done.34.rest_14_.rest_12_.rest_13_
  218.4 15.4 %collective-permute-done.27.rest_7_.rest_5_.rest_6_ = bf16[256,1408]{1,0:T(8,128)(2,1)} collective-permute-done((bf16[256,1408]{1,0:T(8,128)(2,1)}, bf16[256,1408]{1,0:T(8,128)(2,1)}, u32[]{:S(2)}, u32[]{:S(2)}) %collective-permute-start.27) | collective-permute-done | bytes 720928 | tf_op jit(solution)/shard_map/ppermute | solution.py:371
  236.1 10.4 %collective-permute-done.35.rest_15_.rest_13_.rest_14_ = bf16[1408,256]{1,0:T(8,128)(2,1)} collective-permute-done((bf16[1408,256]{1,0:T(8,128)(2,1)}, bf16[1408,256]{1,0:T(8,128)(2,1)}, u32[]{:S(2)}, u32[]{:S(2)}) %collective-permute-start.35) | collective-permute-done | bytes 720928 | tf_op jit(solution)/shard_map/ppermute | solution.py:371
  247.7 1.1 copy-done.7
  248.8 1.1 copy-done.16
  250.0 1.1 copy-done.18
  251.1 1.1 copy-done.21
  252.2 1.1 copy-done.24
  253.3 1.1 copy-done.27
  254.4 8.8 %shard_map.173 = (bf16[384,1024]{1,0:T(8,128)(2,1)S(1)}, bf16[384,1024]{1,0:T(8,128)(2,1)S(1)}, f32[8,1408]{1,0:T(8,128)S(1)}) custom-call(s32[8]{0:T(128)S(1)} %fusion.1.order_ref, f32[2,1024]{1,0:T(2,128)S(1)} %broadcast_select_fusion.gain_ref, f32[3,1408]{1,0:T(4,128)S(1)} %concatenate.17.taps_ref, bf16[384,1024]{1,0:T(8,128)(2,1)} %collective-permute-done.37.rest_0_, ...), custom_call_target="tpu_custom_call" | custom-call | flops 3321888768 | bytes 4194304 | tf_op jit(solution)/shard_map/pallas_call | solution.py:304
  263.7 8.9 %shard_map.174 = (bf16[384,1024]{1,0:T(8,128)(2,1)S(1)}, bf16[384,1024]{1,0:T(8,128)(2,1)S(1)}, f32[8,1408]{1,0:T(8,128)}) custom-call(s32[8]{0:T(128)S(1)} %fusion.1.order_ref, f32[2,1024]{1,0:T(2,128)S(1)} %broadcast_select_fusion.gain_ref, f32[3,1408]{1,0:T(4,128)S(1)} %concatenate.17.taps_ref, f32[8,1408]{1,0:T(8,128)S(1)} %get-tuple-element.32.rest_0_, ...), custom_call_target="tpu_custom_call" | custom-call | flops 3321888768 | bytes 4194304 | tf_op jit(solution)/shard_map/pallas_call | solution.py:304
  272.8 14.3 %shard_map.171 = (bf16[384,1024]{1,0:T(8,128)(2,1)S(1)}, bf16[384,1024]{1,0:T(8,128)(2,1)S(1)}, bf16[384,1024]{1,0:T(8,128)(2,1)S(1)}, bf16[384,1024]{1,0:T(8,128)(2,1)S(1)}, f32[8,1408]{1,0:T(8,128)}) custom-call(s32[8]{0:T(128)S(1)} %fusion.1.order_ref, f32[2,1024]{1,0:T(2,128)S(1)} %broadcast_select_fusion.gain_ref, f32[3,1408]{1,0:T(4,128)S(1)} %concatenate.17.taps_ref, ...), custom_call_target="tpu_custom_call" | custom-call | flops 6643777536 | bytes 4194304 | tf_op jit(solution)/shard_map/pallas_call | solution.py:304
  287.9 1.6 collective-permute-start.45
  291.1 17.4 %collective-permute-done.45.refs_1_ = bf16[384,1024]{1,0:T(8,128)(2,1)S(1)} collective-permute-done((bf16[384,1024]{1,0:T(8,128)(2,1)S(1)}, bf16[384,1024]{1,0:T(8,128)(2,1)S(1)}, u32[]{:S(2)}, u32[]{:S(2)}) %collective-permute-start.45) | collective-permute-done | bytes 786464 | tf_op jit(solution)/shard_map/ppermute | solution.py:363
  308.4 1.1 shard_map.178.refs_2_
  309.5 15.1 %collective-permute-done.42.refs_1_ = bf16[384,1024]{1,0:T(8,128)(2,1)S(1)} collective-permute-done((bf16[384,1024]{1,0:T(8,128)(2,1)S(1)}, bf16[384,1024]{1,0:T(8,128)(2,1)S(1)}, u32[]{:S(2)}, u32[]{:S(2)}) %collective-permute-start.42) | collective-permute-done | bytes 786464 | tf_op jit(solution)/shard_map/ppermute | solution.py:363
  324.6 1.1 shard_map.179
  (168 shorter events, 20.6 us)
Async XLA Ops:
  0.0 152.2 %copy-start = (bf16[1408,256]{1,0:T(8,128)(2,1)S(1)}, bf16[1408,256]{1,0:T(8,128)(2,1)}, u32[]{:S(2)}) copy-start(bf16[1408,256]{1,0:T(8,128)(2,1)} %param.32) | copy-start | bytes 2162692
  0.0 53.4 %copy-start.1 = (bf16[1,768,1024]{2,1,0:T(8,128)(2,1)S(1)}, bf16[1,768,1024]{2,1,0:T(8,128)(2,1)}, u32[]{:S(2)}) copy-start(bf16[1,768,1024]{2,1,0:T(8,128)(2,1)} %param.17) | copy-start | bytes 4718596
  0.0 58.6 %copy-start.47 = (f32[1024]{0:T(1024)S(1)}, f32[1024]{0:T(1024)}, u32[]{:S(2)}) copy-start(f32[1024]{0:T(1024)} %param.24) | copy-start | bytes 12292
  0.0 58.7 %copy-start.46 = (f32[4,1024]{1,0:T(4,128)S(1)}, f32[4,1024]{1,0:T(4,128)}, u32[]{:S(2)}) copy-start(f32[4,1024]{1,0:T(4,128)} %param.21) | copy-start | bytes 49156
  0.0 37.8 %collective-permute-start.16 = (bf16[768,1024]{1,0:T(8,128)(2,1)}, bf16[768,1024]{1,0:T(8,128)(2,1)}, u32[]{:S(2)}, u32[]{:S(2)}) collective-permute-start(bf16[768,1024]{1,0:T(8,128)(2,1)} %bitcast.6), channel_id=1, source_target_pairs={{0,16},{16,0},{1,17},{17,1},{2,18},{18,2},{3,19},{19,3},{4,20},{20... | collective-permute-start | bytes 4718600 | tf_op jit(solution)/shard_map/ppermute | solution.py:363
  3.1 34.7 %copy-start.41 = (bf16[1024,256]{1,0:T(8,128)(2,1)S(1)}, bf16[1024,256]{1,0:T(8,128)(2,1)}, u32[]{:S(2)}) copy-start(bf16[1024,256]{1,0:T(8,128)(2,1)} %param.26) | copy-start | bytes 1572868
  3.1 73.2 %copy-start.48 = (f32[1024]{0:T(1024)S(1)}, f32[1024]{0:T(1024)}, u32[]{:S(2)}) copy-start(f32[1024]{0:T(1024)} %param.25) | copy-start | bytes 12292
  3.1 73.3 %copy-start.42 = (f32[2048]{0:T(1024)S(1)}, f32[2048]{0:T(1024)}, u32[]{:S(2)}) copy-start(f32[2048]{0:T(1024)} %param.18) | copy-start | bytes 24580
  4.2 111.7 %copy-start.9 = (bf16[256,1024]{1,0:T(8,128)(2,1)}, bf16[256,1024]{1,0:T(8,128)(2,1)S(1)}, u32[]{:S(2)}) copy-start(bf16[256,1024]{1,0:T(8,128)(2,1)S(1)} %pad_maximum_fusion.1.rest_2_) | copy-start | bytes 1572868
  4.3 14.4 %collective-permute-start.1 = (bf16[256,1024]{1,0:T(8,128)(2,1)S(1)}, bf16[256,1024]{1,0:T(8,128)(2,1)}, u32[]{:S(2)}, u32[]{:S(2)}) collective-permute-start(bf16[256,1024]{1,0:T(8,128)(2,1)S(1)} %pad_maximum_fusion.1.rest_2_), channel_id=1, source_target_pairs={{0,4},{2,6},{4,12},{6,14},{12,8},{14,10},{8,0},{10,2},{1,5},{3,7},... | collective-permute-start | bytes 1572872 | tf_op jit(solution)/shard_map/ppermute | solution.py:371
  18.7 31.3 %collective-permute-start.2 = (bf16[256,1024]{1,0:T(8,128)(2,1)}, bf16[256,1024]{1,0:T(8,128)(2,1)}, u32[]{:S(2)}, u32[]{:S(2)}) collective-permute-start(bf16[256,1024]{1,0:T(8,128)(2,1)} %collective-permute-done.1.rest_3_), channel_id=1, source_target_pairs={{0,4},{2,6},{4,12},{6,14},{12,8},{14,10},{8,0},{10,2},{1,5},{3,7},... | collective-permute-start | bytes 1572872 | tf_op jit(solution)/shard_map/ppermute | solution.py:371
  37.8 63.5 %collective-permute-start.17 = (bf16[768,1024]{1,0:T(8,128)(2,1)}, bf16[768,1024]{1,0:T(8,128)(2,1)}, u32[]{:S(2)}, u32[]{:S(2)}) collective-permute-start(bf16[768,1024]{1,0:T(8,128)(2,1)} %collective-permute-done.16.rest_0_), channel_id=1, source_target_pairs={{0,1},{1,0},{2,3},{3,2},{4,5},{5,4},{6,7},{7,6},{8,9},{9,8},{10,11... | collective-permute-start | bytes 4718600 | tf_op jit(solution)/shard_map/ppermute | solution.py:366
  37.8 9.9 %collective-permute-start.8 = (bf16[512,256]{1,0:T(8,128)(2,1)S(1)}, bf16[512,256]{1,0:T(8,128)(2,1)S(1)}, u32[]{:S(2)}, u32[]{:S(2)}) collective-permute-start(bf16[512,256]{1,0:T(8,128)(2,1)S(1)} %constant_dynamic-slice_fusion.9.rest_0_), channel_id=1, source_target_pairs={{0,4},{2,6},{4,12},{6,14},{12,8},{14,10},{8,0},{10,2},{1,5},{3,7},... | collective-permute-start | bytes 786440 | tf_op jit(solution)/shard_map/ppermute | solution.py:371
  47.7 68.3 %copy-start.29 = (bf16[512,256]{1,0:T(8,128)(2,1)}, bf16[512,256]{1,0:T(8,128)(2,1)S(1)}, u32[]{:S(2)}) copy-start(bf16[512,256]{1,0:T(8,128)(2,1)S(1)} %collective-permute-done.8.rest_1_) | copy-start | bytes 786436
  47.7 10.2 %collective-permute-start.9 = (bf16[512,256]{1,0:T(8,128)(2,1)S(1)}, bf16[512,256]{1,0:T(8,128)(2,1)}, u32[]{:S(2)}, u32[]{:S(2)}) collective-permute-start(bf16[512,256]{1,0:T(8,128)(2,1)S(1)} %collective-permute-done.8.rest_1_), channel_id=1, source_target_pairs={{0,4},{2,6},{4,12},{6,14},{12,8},{14,10},{8,0},{10,2},{1,5},{3,7},... | collective-permute-start | bytes 786440 | tf_op jit(solution)/shard_map/ppermute | solution.py:371
  48.5 13.3 %collective-permute-start.4 = (bf16[256,1024]{1,0:T(8,128)(2,1)S(1)}, bf16[256,1024]{1,0:T(8,128)(2,1)}, u32[]{:S(2)}, u32[]{:S(2)}) collective-permute-start(bf16[256,1024]{1,0:T(8,128)(2,1)S(1)} %pad_maximum_fusion.1.rest_2_), channel_id=1, source_target_pairs={{0,2},{2,0},{4,6},{6,4},{8,10},{10,8},{12,14},{14,12},{1,3},{3,1},... | collective-permute-start | bytes 1572872 | tf_op jit(solution)/shard_map/ppermute | solution.py:378
  50.0 24.9 %collective-permute-start.3 = (bf16[256,1024]{1,0:T(8,128)(2,1)}, bf16[256,1024]{1,0:T(8,128)(2,1)}, u32[]{:S(2)}, u32[]{:S(2)}) collective-permute-start(bf16[256,1024]{1,0:T(8,128)(2,1)} %collective-permute-done.2.rest_4_), channel_id=1, source_target_pairs={{0,4},{2,6},{4,12},{6,14},{12,8},{14,10},{8,0},{10,2},{1,5},{3,7},... | collective-permute-start | bytes 1572872 | tf_op jit(solution)/shard_map/ppermute | solution.py:371
  53.4 79.0 %collective-permute-start = (bf16[768,1024]{1,0:T(8,128)(2,1)S(1)}, bf16[768,1024]{1,0:T(8,128)(2,1)}, u32[]{:S(2)}, u32[]{:S(2)}) collective-permute-start(bf16[768,1024]{1,0:T(8,128)(2,1)S(1)} %bitcast.7), channel_id=1, source_target_pairs={{0,1},{1,0},{2,3},{3,2},{4,5},{5,4},{6,7},{7,6},{8,9},{9,8},{10,11... | collective-permute-start | bytes 4718600 | tf_op jit(solution)/shard_map/ppermute | solution.py:366
  57.8 15.7 %collective-permute-start.10 = (bf16[512,256]{1,0:T(8,128)(2,1)}, bf16[512,256]{1,0:T(8,128)(2,1)}, u32[]{:S(2)}, u32[]{:S(2)}) collective-permute-start(bf16[512,256]{1,0:T(8,128)(2,1)} %collective-permute-done.9.rest_2_), channel_id=1, source_target_pairs={{0,4},{2,6},{4,12},{6,14},{12,8},{14,10},{8,0},{10,2},{1,5},{3,7},... | collective-permute-start | bytes 786440 | tf_op jit(solution)/shard_map/ppermute | solution.py:371
  61.8 18.2 %collective-permute-start.5 = (bf16[256,1024]{1,0:T(8,128)(2,1)}, bf16[256,1024]{1,0:T(8,128)(2,1)}, u32[]{:S(2)}, u32[]{:S(2)}) collective-permute-start(bf16[256,1024]{1,0:T(8,128)(2,1)} %collective-permute-done.1.rest_3_), channel_id=1, source_target_pairs={{0,2},{2,0},{4,6},{6,4},{8,10},{10,8},{12,14},{14,12},{1,3},{3,1},... | collective-permute-start | bytes 1572872 | tf_op jit(solution)/shard_map/ppermute | solution.py:378
  73.6 15.1 %collective-permute-start.6 = (bf16[256,1024]{1,0:T(8,128)(2,1)}, bf16[256,1024]{1,0:T(8,128)(2,1)}, u32[]{:S(2)}, u32[]{:S(2)}) collective-permute-start(bf16[256,1024]{1,0:T(8,128)(2,1)} %collective-permute-done.2.rest_4_), channel_id=1, source_target_pairs={{0,2},{2,0},{4,6},{6,4},{8,10},{10,8},{12,14},{14,12},{1,3},{3,1},... | collective-permute-start | bytes 1572872 | tf_op jit(solution)/shard_map/ppermute | solution.py:378
  75.0 25.0 %collective-permute-start.7 = (bf16[256,1024]{1,0:T(8,128)(2,1)}, bf16[256,1024]{1,0:T(8,128)(2,1)}, u32[]{:S(2)}, u32[]{:S(2)}) collective-permute-start(bf16[256,1024]{1,0:T(8,128)(2,1)} %collective-permute-done.3.rest_5_), channel_id=1, source_target_pairs={{0,2},{2,0},{4,6},{6,4},{8,10},{10,8},{12,14},{14,12},{1,3},{3,1},... | collective-permute-start | bytes 1572872 | tf_op jit(solution)/shard_map/ppermute | solution.py:378
  77.6 38.4 %copy-start.11 = (bf16[4,128,256]{2,1,0:T(8,128)(2,1)}, bf16[4,128,256]{2,1,0:T(8,128)(2,1)S(1)}, u32[]{:S(2)}) copy-start(bf16[4,128,256]{2,1,0:T(8,128)(2,1)S(1)} %pad_maximum_fusion.2.gates_ref) | copy-start | bytes 786436
  80.0 36.0 %collective-permute-start.11 = (bf16[512,256]{1,0:T(8,128)(2,1)S(1)}, bf16[512,256]{1,0:T(8,128)(2,1)S(1)}, u32[]{:S(2)}, u32[]{:S(2)}) collective-permute-start(bf16[512,256]{1,0:T(8,128)(2,1)S(1)} %constant_dynamic-slice_fusion.9.rest_0_), channel_id=1, source_target_pairs={{0,2},{2,0},{4,6},{6,4},{8,10},{10,8},{12,14},{14,12},{1,3},{3,1},... | collective-permute-start | bytes 786440 | tf_op jit(solution)/shard_map/ppermute | solution.py:378
  88.7 27.3 %collective-permute-start.12 = (bf16[512,256]{1,0:T(8,128)(2,1)S(1)}, bf16[512,256]{1,0:T(8,128)(2,1)S(1)}, u32[]{:S(2)}, u32[]{:S(2)}) collective-permute-start(bf16[512,256]{1,0:T(8,128)(2,1)S(1)} %collective-permute-done.8.rest_1_), channel_id=1, source_target_pairs={{0,2},{2,0},{4,6},{6,4},{8,10},{10,8},{12,14},{14,12},{1,3},{3,1},... | collective-permute-start | bytes 786440 | tf_op jit(solution)/shard_map/ppermute | solution.py:378
  99.9 16.7 %collective-permute-start.13 = (bf16[512,256]{1,0:T(8,128)(2,1)}, bf16[512,256]{1,0:T(8,128)(2,1)S(1)}, u32[]{:S(2)}, u32[]{:S(2)}) collective-permute-start(bf16[512,256]{1,0:T(8,128)(2,1)} %collective-permute-done.9.rest_2_), channel_id=1, source_target_pairs={{0,2},{2,0},{4,6},{6,4},{8,10},{10,8},{12,14},{14,12},{1,3},{3,1},... | collective-permute-start | bytes 786440 | tf_op jit(solution)/shard_map/ppermute | solution.py:378
  101.3 19.0 %collective-permute-start.14 = (bf16[512,256]{1,0:T(8,128)(2,1)}, bf16[512,256]{1,0:T(8,128)(2,1)S(1)}, u32[]{:S(2)}, u32[]{:S(2)}) collective-permute-start(bf16[512,256]{1,0:T(8,128)(2,1)} %collective-permute-done.10.rest_3_), channel_id=1, source_target_pairs={{0,2},{2,0},{4,6},{6,4},{8,10},{10,8},{12,14},{14,12},{1,3},{3,1},... | collective-permute-start | bytes 786440 | tf_op jit(solution)/shard_map/ppermute | solution.py:378
  127.1 26.7 %collective-permute-start.21 = (bf16[384,1024]{1,0:T(8,128)(2,1)}, bf16[384,1024]{1,0:T(8,128)(2,1)}, u32[]{:S(2)}, u32[]{:S(2)}) collective-permute-start(bf16[384,1024]{1,0:T(8,128)(2,1)} %get-tuple-element.29), channel_id=1, source_target_pairs={{0,1},{1,0},{2,3},{3,2},{4,5},{5,4},{6,7},{7,6},{8,9},{9,8},{10,11... | collective-permute-start | bytes 2359304 | tf_op jit(solution)/shard_map/ppermute | solution.py:366
  130.1 34.6 %collective-permute-start.25 = (bf16[256,1408]{1,0:T(8,128)(2,1)}, bf16[256,1408]{1,0:T(8,128)(2,1)S(1)}, u32[]{:S(2)}, u32[]{:S(2)}) collective-permute-start(bf16[256,1408]{1,0:T(8,128)(2,1)} %concatenate.18.rest_4_.rest_2_.rest_3_), channel_id=1, source_target_pairs={{0,4},{2,6},{4,12},{6,14},{12,8},{14,10},{8,0},{10,2},{1,5},{3,7},... | collective-permute-start | bytes 2162696 | tf_op jit(solution)/shard_map/ppermute | solution.py:371
  134.4 13.7 %copy-start.39 = (bf16[512,256]{1,0:T(8,128)(2,1)S(1)}, bf16[512,256]{1,0:T(8,128)(2,1)}, u32[]{:S(2)}) copy-start(bf16[512,256]{1,0:T(8,128)(2,1)} %copy-done.38) | copy-start | bytes 786436
  151.6 14.6 %collective-permute-start.20 = (bf16[384,1024]{1,0:T(8,128)(2,1)S(1)}, bf16[384,1024]{1,0:T(8,128)(2,1)S(1)}, u32[]{:S(2)}, u32[]{:S(2)}) collective-permute-start(bf16[384,1024]{1,0:T(8,128)(2,1)S(1)} %get-tuple-element.27), channel_id=1, source_target_pairs={{0,1},{1,0},{2,3},{3,2},{4,5},{5,4},{6,7},{7,6},{8,9},{9,8},{10,11... | collective-permute-start | bytes 2359304 | tf_op jit(solution)/shard_map/ppermute | solution.py:366
  151.9 12.5 %collective-permute-start.18 = (bf16[384,1024]{1,0:T(8,128)(2,1)S(1)}, bf16[384,1024]{1,0:T(8,128)(2,1)S(1)}, u32[]{:S(2)}, u32[]{:S(2)}) collective-permute-start(bf16[384,1024]{1,0:T(8,128)(2,1)S(1)} %copy-done.14), channel_id=1, source_target_pairs={{0,1},{1,0},{2,3},{3,2},{4,5},{5,4},{6,7},{7,6},{8,9},{9,8},{10,11... | collective-permute-start | bytes 2359304 | tf_op jit(solution)/shard_map/ppermute | solution.py:366
  152.2 10.6 %collective-permute-start.32 = (bf16[704,256]{1,0:T(8,128)(2,1)S(1)}, bf16[704,256]{1,0:T(8,128)(2,1)S(1)}, u32[]{:S(2)}, u32[]{:S(2)}) collective-permute-start(bf16[704,256]{1,0:T(8,128)(2,1)S(1)} %constant_dynamic-slice_fusion.4), channel_id=1, source_target_pairs={{0,2},{2,0},{4,6},{6,4},{8,10},{10,8},{12,14},{14,12},{1,3},{3,1},... | collective-permute-start | bytes 1081352 | tf_op jit(solution)/shard_map/ppermute | solution.py:381
  155.2 20.5 %copy-start.6 = (bf16[256,1408]{1,0:T(8,128)(2,1)S(1)}, bf16[256,1408]{1,0:T(8,128)(2,1)}, u32[]{:S(2)}) copy-start(bf16[256,1408]{1,0:T(8,128)(2,1)} %concatenate.18.rest_4_.rest_2_.rest_3_) | copy-start | bytes 2162692
  155.2 20.5 %collective-permute-start.22 = (bf16[384,1024]{1,0:T(8,128)(2,1)S(1)}, bf16[384,1024]{1,0:T(8,128)(2,1)S(1)}, u32[]{:S(2)}, u32[]{:S(2)}) collective-permute-start(bf16[384,1024]{1,0:T(8,128)(2,1)S(1)} %shard_map.169), channel_id=1, source_target_pairs={{0,16},{16,0},{1,17},{17,1},{2,18},{18,2},{3,19},{19,3},{4,20},{20... | collective-permute-start | bytes 2359304 | tf_op jit(solution)/shard_map/ppermute | solution.py:363
  162.9 13.8 %copy-start.40 = (bf16[1408,256]{1,0:T(8,128)(2,1)}, bf16[1408,256]{1,0:T(8,128)(2,1)S(1)}, u32[]{:S(2)}) copy-start(bf16[1408,256]{1,0:T(8,128)(2,1)S(1)} %pad_maximum_fusion.rest_12_.rest_10_.rest_11_) | copy-start | bytes 2162692
  162.9 20.0 %collective-permute-start.33 = (bf16[1408,256]{1,0:T(8,128)(2,1)S(1)}, bf16[1408,256]{1,0:T(8,128)(2,1)S(1)}, u32[]{:S(2)}, u32[]{:S(2)}) collective-permute-start(bf16[1408,256]{1,0:T(8,128)(2,1)S(1)} %pad_maximum_fusion.rest_12_.rest_10_.rest_11_), channel_id=1, source_target_pairs={{0,4},{2,6},{4,12},{6,14},{12,8},{14,10},{8,0},{10,2},{1,5},{3,7},... | collective-permute-start | bytes 2162696 | tf_op jit(solution)/shard_map/ppermute | solution.py:371
  164.4 33.9 %collective-permute-start.15 = (bf16[384,1024]{1,0:T(8,128)(2,1)S(1)}, bf16[384,1024]{1,0:T(8,128)(2,1)S(1)}, u32[]{:S(2)}, u32[]{:S(2)}) collective-permute-start(bf16[384,1024]{1,0:T(8,128)(2,1)S(1)} %get-tuple-element.23), channel_id=1, source_target_pairs={{0,1},{1,0},{2,3},{3,2},{4,5},{5,4},{6,7},{7,6},{8,9},{9,8},{10,11... | collective-permute-start | bytes 2359304 | tf_op jit(solution)/shard_map/ppermute | solution.py:366
  164.7 32.2 %copy-start.17 = (bf16[256,1408]{1,0:T(8,128)(2,1)}, bf16[256,1408]{1,0:T(8,128)(2,1)S(1)}, u32[]{:S(2)}) copy-start(bf16[256,1408]{1,0:T(8,128)(2,1)S(1)} %collective-permute-done.25.rest_5_.rest_3_.rest_4_) | copy-start | bytes 2162692
  164.7 34.2 %collective-permute-start.19 = (bf16[384,1024]{1,0:T(8,128)(2,1)S(1)}, bf16[384,1024]{1,0:T(8,128)(2,1)S(1)}, u32[]{:S(2)}, u32[]{:S(2)}) collective-permute-start(bf16[384,1024]{1,0:T(8,128)(2,1)S(1)} %shard_map.167), channel_id=1, source_target_pairs={{0,16},{16,0},{1,17},{17,1},{2,18},{18,2},{3,19},{19,3},{4,20},{20... | collective-permute-start | bytes 2359304 | tf_op jit(solution)/shard_map/ppermute | solution.py:363
  166.2 30.6 %collective-permute-start.26 = (bf16[256,1408]{1,0:T(8,128)(2,1)S(1)}, bf16[256,1408]{1,0:T(8,128)(2,1)}, u32[]{:S(2)}, u32[]{:S(2)}) collective-permute-start(bf16[256,1408]{1,0:T(8,128)(2,1)S(1)} %collective-permute-done.25.rest_5_.rest_3_.rest_4_), channel_id=1, source_target_pairs={{0,4},{2,6},{4,12},{6,14},{12,8},{14,10},{8,0},{10,2},{1,5},{3,7},... | collective-permute-start | bytes 2162696 | tf_op jit(solution)/shard_map/ppermute | solution.py:371
  175.7 25.1 %collective-permute-start.28 = (bf16[256,1408]{1,0:T(8,128)(2,1)S(1)}, bf16[256,1408]{1,0:T(8,128)(2,1)S(1)}, u32[]{:S(2)}, u32[]{:S(2)}) collective-permute-start(bf16[256,1408]{1,0:T(8,128)(2,1)S(1)} %copy-done.6), channel_id=1, source_target_pairs={{0,2},{2,0},{4,6},{6,4},{8,10},{10,8},{12,14},{14,12},{1,3},{3,1},... | collective-permute-start | bytes 2162696 | tf_op jit(solution)/shard_map/ppermute | solution.py:378
  182.9 17.9 %copy-start.49 = (bf16[1408,256]{1,0:T(8,128)(2,1)}, bf16[1408,256]{1,0:T(8,128)(2,1)S(1)}, u32[]{:S(2)}) copy-start(bf16[1408,256]{1,0:T(8,128)(2,1)S(1)} %collective-permute-done.33.rest_13_.rest_11_.rest_12_) | copy-start | bytes 2162692
  182.9 26.6 %collective-permute-start.37 = (bf16[384,1024]{1,0:T(8,128)(2,1)S(1)}, bf16[384,1024]{1,0:T(8,128)(2,1)}, u32[]{:S(2)}, u32[]{:S(2)}) collective-permute-start(bf16[384,1024]{1,0:T(8,128)(2,1)S(1)} %shard_map.170.rest_0_.refs_0_), channel_id=1, source_target_pairs={{0,16},{16,0},{1,17},{17,1},{2,18},{18,2},{3,19},{19,3},{4,20},{20... | collective-permute-start | bytes 2359304 | tf_op jit(solution)/shard_map/ppermute | solution.py:363
  196.8 16.6 %collective-permute-start.29 = (bf16[256,1408]{1,0:T(8,128)(2,1)S(1)}, bf16[256,1408]{1,0:T(8,128)(2,1)S(1)}, u32[]{:S(2)}, u32[]{:S(2)}) collective-permute-start(bf16[256,1408]{1,0:T(8,128)(2,1)S(1)} %collective-permute-done.25.rest_5_.rest_3_.rest_4_), channel_id=1, source_target_pairs={{0,2},{2,0},{4,6},{6,4},{8,10},{10,8},{12,14},{14,12},{1,3},{3,1},... | collective-permute-start | bytes 2162696 | tf_op jit(solution)/shard_map/ppermute | solution.py:378
  198.3 20.0 %collective-permute-start.34 = (bf16[1408,256]{1,0:T(8,128)(2,1)S(1)}, bf16[1408,256]{1,0:T(8,128)(2,1)}, u32[]{:S(2)}, u32[]{:S(2)}) collective-permute-start(bf16[1408,256]{1,0:T(8,128)(2,1)S(1)} %collective-permute-done.33.rest_13_.rest_11_.rest_12_), channel_id=1, source_target_pairs={{0,4},{2,6},{4,12},{6,14},{12,8},{14,10},{8,0},{10,2},{1,5},{3,7},... | collective-permute-start | bytes 2162696 | tf_op jit(solution)/shard_map/ppermute | solution.py:371
  198.9 34.9 %collective-permute-start.27 = (bf16[256,1408]{1,0:T(8,128)(2,1)}, bf16[256,1408]{1,0:T(8,128)(2,1)}, u32[]{:S(2)}, u32[]{:S(2)}) collective-permute-start(bf16[256,1408]{1,0:T(8,128)(2,1)} %collective-permute-done.26.rest_6_.rest_4_.rest_5_), channel_id=1, source_target_pairs={{0,4},{2,6},{4,12},{6,14},{12,8},{14,10},{8,0},{10,2},{1,5},{3,7},... | collective-permute-start | bytes 2162696 | tf_op jit(solution)/shard_map/ppermute | solution.py:371
  200.3 34.0 %copy-start.43 = (f32[2048]{0:T(1024)S(1)}, f32[2048]{0:T(1024)}, u32[]{:S(2)}) copy-start(f32[2048]{0:T(1024)} %param.27) | copy-start | bytes 24580
  200.3 34.3 %copy-start.44 = (f32[3,1408]{1,0:T(4,128)S(1)}, f32[3,1408]{1,0:T(4,128)}, u32[]{:S(2)}) copy-start(f32[3,1408]{1,0:T(4,128)} %param.31) | copy-start | bytes 50692
  200.3 34.3 %copy-start.45 = (f32[3,1408]{1,0:T(4,128)S(1)}, f32[3,1408]{1,0:T(4,128)}, u32[]{:S(2)}) copy-start(f32[3,1408]{1,0:T(4,128)} %param.30) | copy-start | bytes 50692
  201.7 32.6 %collective-permute-start.39 = (bf16[384,1024]{1,0:T(8,128)(2,1)S(1)}, bf16[384,1024]{1,0:T(8,128)(2,1)}, u32[]{:S(2)}, u32[]{:S(2)}) collective-permute-start(bf16[384,1024]{1,0:T(8,128)(2,1)S(1)} %shard_map.168.rest_1_.refs_0_), channel_id=1, source_target_pairs={{0,16},{16,0},{1,17},{17,1},{2,18},{18,2},{3,19},{19,3},{4,20},{20... | collective-permute-start | bytes 2359304 | tf_op jit(solution)/shard_map/ppermute | solution.py:363
  209.5 37.3 %collective-permute-start.38 = (bf16[384,1024]{1,0:T(8,128)(2,1)}, bf16[384,1024]{1,0:T(8,128)(2,1)S(1)}, u32[]{:S(2)}, u32[]{:S(2)}) collective-permute-start(bf16[384,1024]{1,0:T(8,128)(2,1)} %collective-permute-done.37.rest_0_), channel_id=1, source_target_pairs={{0,1},{1,0},{2,3},{3,2},{4,5},{5,4},{6,7},{7,6},{8,9},{9,8},{10,11... | collective-permute-start | bytes 2359304 | tf_op jit(solution)/shard_map/ppermute | solution.py:366
  214.2 20.5 %collective-permute-start.30 = (bf16[256,1408]{1,0:T(8,128)(2,1)}, bf16[256,1408]{1,0:T(8,128)(2,1)S(1)}, u32[]{:S(2)}, u32[]{:S(2)}) collective-permute-start(bf16[256,1408]{1,0:T(8,128)(2,1)} %collective-permute-done.26.rest_6_.rest_4_.rest_5_), channel_id=1, source_target_pairs={{0,2},{2,0},{4,6},{6,4},{8,10},{10,8},{12,14},{14,12},{1,3},{3,1},... | collective-permute-start | bytes 2162696 | tf_op jit(solution)/shard_map/ppermute | solution.py:378
  218.4 28.2 %collective-permute-start.35 = (bf16[1408,256]{1,0:T(8,128)(2,1)}, bf16[1408,256]{1,0:T(8,128)(2,1)}, u32[]{:S(2)}, u32[]{:S(2)}) collective-permute-start(bf16[1408,256]{1,0:T(8,128)(2,1)} %collective-permute-done.34.rest_14_.rest_12_.rest_13_), channel_id=1, source_target_pairs={{0,4},{2,6},{4,12},{6,14},{12,8},{14,10},{8,0},{10,2},{1,5},{3,7},... | collective-permute-start | bytes 2162696 | tf_op jit(solution)/shard_map/ppermute | solution.py:371
  233.8 13.0 %collective-permute-start.31 = (bf16[256,1408]{1,0:T(8,128)(2,1)}, bf16[256,1408]{1,0:T(8,128)(2,1)}, u32[]{:S(2)}, u32[]{:S(2)}) collective-permute-start(bf16[256,1408]{1,0:T(8,128)(2,1)} %collective-permute-done.27.rest_7_.rest_5_.rest_6_), channel_id=1, source_target_pairs={{0,2},{2,0},{4,6},{6,4},{8,10},{10,8},{12,14},{14,12},{1,3},{3,1},... | collective-permute-start | bytes 2162696 | tf_op jit(solution)/shard_map/ppermute | solution.py:378
  234.3 29.3 %collective-permute-start.40 = (bf16[384,1024]{1,0:T(8,128)(2,1)}, bf16[384,1024]{1,0:T(8,128)(2,1)}, u32[]{:S(2)}, u32[]{:S(2)}) collective-permute-start(bf16[384,1024]{1,0:T(8,128)(2,1)} %collective-permute-done.39.rest_1_), channel_id=1, source_target_pairs={{0,1},{1,0},{2,3},{3,2},{4,5},{5,4},{6,7},{7,6},{8,9},{9,8},{10,11... | collective-permute-start | bytes 2359304 | tf_op jit(solution)/shard_map/ppermute | solution.py:366
  235.6 37.2 %collective-permute-start.23 = (bf16[384,1024]{1,0:T(8,128)(2,1)S(1)}, bf16[384,1024]{1,0:T(8,128)(2,1)}, u32[]{:S(2)}, u32[]{:S(2)}) collective-permute-start(bf16[384,1024]{1,0:T(8,128)(2,1)S(1)} %shard_map.170.rest_0_.refs_0_), channel_id=1, source_target_pairs={{0,1},{1,0},{2,3},{3,2},{4,5},{5,4},{6,7},{7,6},{8,9},{9,8},{10,11... | collective-permute-start | bytes 2359304 | tf_op jit(solution)/shard_map/ppermute | solution.py:366
  246.5 26.3 %collective-permute-start.24 = (bf16[384,1024]{1,0:T(8,128)(2,1)}, bf16[384,1024]{1,0:T(8,128)(2,1)}, u32[]{:S(2)}, u32[]{:S(2)}) collective-permute-start(bf16[384,1024]{1,0:T(8,128)(2,1)} %copy-done.2), channel_id=1, source_target_pairs={{0,1},{1,0},{2,3},{3,2},{4,5},{5,4},{6,7},{7,6},{8,9},{9,8},{10,11... | collective-permute-start | bytes 2359304 | tf_op jit(solution)/shard_map/ppermute | solution.py:366
  263.3 24.4 %collective-permute-start.44 = (bf16[384,1024]{1,0:T(8,128)(2,1)S(1)}, bf16[384,1024]{1,0:T(8,128)(2,1)S(1)}, u32[]{:S(2)}, u32[]{:S(2)}) collective-permute-start(bf16[384,1024]{1,0:T(8,128)(2,1)S(1)} %get-tuple-element.38), channel_id=1, source_target_pairs={{0,1},{1,0},{2,3},{3,2},{4,5},{5,4},{6,7},{7,6},{8,9},{9,8},{10,11... | collective-permute-start | bytes 2359304 | tf_op jit(solution)/shard_map/ppermute | solution.py:366
  272.6 16.9 %collective-permute-start.41 = (bf16[384,1024]{1,0:T(8,128)(2,1)S(1)}, bf16[384,1024]{1,0:T(8,128)(2,1)S(1)}, u32[]{:S(2)}, u32[]{:S(2)}) collective-permute-start(bf16[384,1024]{1,0:T(8,128)(2,1)S(1)} %get-tuple-element.34), channel_id=1, source_target_pairs={{0,1},{1,0},{2,3},{3,2},{4,5},{5,4},{6,7},{7,6},{8,9},{9,8},{10,11... | collective-permute-start | bytes 2359304 | tf_op jit(solution)/shard_map/ppermute | solution.py:366
  287.1 3.2 collective-permute-start.43
  287.5 3.2 collective-permute-start.36
  287.9 20.5 %collective-permute-start.45 = (bf16[384,1024]{1,0:T(8,128)(2,1)S(1)}, bf16[384,1024]{1,0:T(8,128)(2,1)S(1)}, u32[]{:S(2)}, u32[]{:S(2)}) collective-permute-start(bf16[384,1024]{1,0:T(8,128)(2,1)S(1)} %shard_map.177), channel_id=1, source_target_pairs={{0,16},{16,0},{1,17},{17,1},{2,18},{18,2},{3,19},{19,3},{4,20},{20... | collective-permute-start | bytes 2359304 | tf_op jit(solution)/shard_map/ppermute | solution.py:363
  289.7 34.9 %collective-permute-start.42 = (bf16[384,1024]{1,0:T(8,128)(2,1)S(1)}, bf16[384,1024]{1,0:T(8,128)(2,1)S(1)}, u32[]{:S(2)}, u32[]{:S(2)}) collective-permute-start(bf16[384,1024]{1,0:T(8,128)(2,1)S(1)} %shard_map.175), channel_id=1, source_target_pairs={{0,16},{16,0},{1,17},{17,1},{2,18},{18,2},{3,19},{19,3},{4,20},{20... | collective-permute-start | bytes 2359304 | tf_op jit(solution)/shard_map/ppermute | solution.py:363
  (32 other events, 174.4 us)
